TPU v7x, 32 devices: a whole 2x2x4 slice. The times are simulated.
32 devices in a mesh: fs: 8 (over z, x), tp: 4 (over y, core).
Axes of the slice: x: 2, y: 2, z: 4, core: 2. Of those that a mesh axis runs over, the one named last changes fastest.
Arguments:
- tokens: bfloat16 [3072, 4096], P('fs', 'tp'), may hold values from -600 to 600
- gate_master: float32 [8, 4096, 512], P(None, 'fs', 'tp'), may hold values from -0.09375 to 0.09375
- up_master: float32 [8, 4096, 512], P(None, 'fs', 'tp'), may hold values from -0.09375 to 0.09375
- down_master: float32 [8, 4096, 512], P(None, 'fs', 'tp'), may hold values from -0.25 to 0.25
- norm_gain: float32 [4096], P('fs'), may hold values from 0.1 to 1.9
- routes: int32 [3072, 2], P('fs'), may hold values from 0 to 7, all different within a row; in each aligned block of 384 rows (0 to 383, 384 to 767, ...) at most 192 rows name the same one
- route_weight: float32 [3072, 2], P('fs'), may hold values from 0.1 to 1
Outputs:
- gate_out: bfloat16 [8, 4096, 512], P('fs', None, 'tp')
- up_out: bfloat16 [8, 4096, 512], P('fs', None, 'tp')
- down_out: bfloat16 [8, 4096, 512], P('fs', None, 'tp')
- mixed: bfloat16 [3072, 4096], P('fs', 'tp')
Inputs may be any that keep to these rules, and one draw needn't show every extreme that they name: `routes`: within the rows of one index of fs no expert is named by more than 192 pairs, a bound that some block reaches; the 2 experts of a row differ.
All inputs are finite; a program needn't handle non-finite values.
Results may differ from a plain program's by a relative error of at most 0.0087.
Values may be sent and summed in bfloat16 or wider, within the bound.
A program may use at most 128 MiB of HBM per device.

v0:
```python
import jax
import jax.numpy as jnp
from jax import lax
from jax.sharding import PartitionSpec as P

norm_eps = 1e-06


def slot_table(expert_ids, n_experts, capacity, top_count):
    assigned = expert_ids.shape[0]
    onehot = (expert_ids[:, None] == jnp.arange(n_experts, dtype=jnp.int32)[None, :]).astype(
        jnp.int32
    )
    before = jnp.cumsum(onehot, axis=0) - onehot
    slots = jnp.sum(before * onehot, axis=1)
    position = expert_ids * capacity + slots
    owners = jnp.arange(assigned, dtype=jnp.int32) // top_count
    matches = position[None, :] == jnp.arange(n_experts * capacity, dtype=jnp.int32)[:, None]
    slot_token = jnp.max(jnp.where(matches, owners[None, :], -1), axis=1)
    return (position, slot_token)


def place_rows(normed, slot_token):
    padded = jnp.concatenate([normed, jnp.zeros((1, normed.shape[1]), normed.dtype)], axis=0)
    chosen = jnp.where(slot_token < 0, normed.shape[0], slot_token)
    return padded[chosen]


def body(tokens, gate_master, up_master, down_master, norm_gain, routes, route_weight):
    n_experts = gate_master.shape[0]
    tok_rows = routes.shape[0]
    top_count = routes.shape[1]
    capacity = 2 * tok_rows * top_count // n_experts
    folded = norm_gain[None, :, None]
    gate_cast = (gate_master * folded).astype(jnp.bfloat16)
    up_cast = (up_master * folded).astype(jnp.bfloat16)
    down_cast = down_master.astype(jnp.bfloat16)
    gate_out, up_out, down_out = (
        lax.all_to_all(gate_cast, "fs", split_axis=0, concat_axis=1, tiled=True),
        lax.all_to_all(up_cast, "fs", split_axis=0, concat_axis=1, tiled=True),
        lax.all_to_all(down_cast, "fs", split_axis=0, concat_axis=1, tiled=True),
    )
    flat_routes = routes.reshape(-1)
    position, slot_token = slot_table(flat_routes, n_experts, capacity, top_count)
    mix_weights = route_weight / jnp.sum(route_weight, axis=1, keepdims=True)
    gate_mat = gate_out[0]
    up_mat = up_out[0]
    token_float = tokens.astype(jnp.float32)
    full_width = token_float.shape[1] * lax.axis_size("tp")
    sumsquares = lax.psum(jnp.sum(token_float * token_float, axis=1), "tp")
    inverse = lax.rsqrt(sumsquares / full_width + norm_eps)[:, None]
    normed = (token_float * inverse).astype(jnp.bfloat16)
    outgoing = place_rows(normed, slot_token).reshape(n_experts, capacity, normed.shape[1])
    arrived = lax.all_to_all(outgoing, "fs", split_axis=0, concat_axis=0, tiled=True).reshape(
        -1, normed.shape[1]
    )
    segment = lax.all_gather(arrived, "tp", axis=1, tiled=True)
    gate_val = jnp.dot(segment, gate_mat, preferred_element_type=jnp.float32)
    up_val = jnp.dot(segment, up_mat, preferred_element_type=jnp.float32)
    hidden = (jax.nn.silu(gate_val) * up_val).astype(jnp.bfloat16)
    hidden_whole = lax.all_gather(hidden, "tp", axis=1, tiled=True)
    down_quarter = lax.all_to_all(down_out[0], "tp", split_axis=0, concat_axis=1, tiled=True)
    result = lax.dot_general(
        hidden_whole, down_quarter, (((1,), (1,)), ((), ())), preferred_element_type=jnp.float32
    )
    summed = result.astype(jnp.bfloat16)
    returned = lax.all_to_all(
        summed.reshape(-1, capacity, summed.shape[1]), "fs", split_axis=0, concat_axis=0, tiled=True
    )
    flat_back = returned.reshape(-1, summed.shape[1])
    picked = flat_back[position].astype(jnp.float32).reshape(tok_rows, top_count, summed.shape[1])
    mixed = jnp.sum(mix_weights[:, :, None] * picked, axis=1).astype(jnp.bfloat16)
    return (gate_out, up_out, down_out, mixed)


def solution(mesh):
    placed = (
        P("fs", "tp"),
        P(None, "fs", "tp"),
        P(None, "fs", "tp"),
        P(None, "fs", "tp"),
        P("fs"),
        P("fs", None),
        P("fs", None),
    )
    return jax.shard_map(
        body,
        mesh=mesh,
        in_specs=placed,
        out_specs=(P("fs", None, "tp"), P("fs", None, "tp"), P("fs", None, "tp"), P("fs", "tp")),
        check_vma=False,
    )
```

profile of v0, /device:TPU:0, one launch (start us, length us, event | category | flops | bytes accessed | tf_op | source)
XLA Modules:
  0.0 341.4 jit_solution(13418795608480970905)
XLA Ops:
  8.3 1.7 reduce-window.6
  11.4 1.4 fusion.1
  12.7 8.4 %psum.7 = f32[384]{0:T(512)S(1)} all-reduce(f32[384]{0:T(512)S(1)} %fusion.1), channel_id=1, replica_groups=mesh['fs'=8,'tp'=4] {'tp'}, use_global_device_ids=true, to_apply=%region_2.3 | all-reduce | flops 384 | bytes 3072 | tf_op jit(solution)/shard_map/psum | solution.py:50
  21.1 1.3 fusion.2
  22.5 5.8 %gather_fusion = bf16[1536,1024]{1,0:T(8,128)(2,1)} fusion(bf16[385,1024]{1,0:T(8,128)(2,1)S(1)} %concatenate.3, s32[2048]{0:T(1024)S(1)} %pad_clamp_fusion), kind=kCustom, calls=%fused_computation | custom fusion | bytes 6297600 | tf_op jit(solution)/shard_map/gather | solution.py:26
  28.4 75.4 %all_to_all.65 = bf16[8,192,1024]{2,1,0:T(8,128)(2,1)} all-to-all(bf16[8,192,1024]{2,1,0:T(8,128)(2,1)} %bitcast.30), channel_id=1, replica_groups=mesh['fs'=8,'tp'=4] {'fs'}, dimensions={0} | all-to-all | bytes 6291456 | tf_op jit(solution)/shard_map/all_to_all | solution.py:54
  103.8 1.6 copy-done.6
  105.4 3.0 multiply_convert_fusion
  108.3 28.8 %all_to_all.66 = bf16[8,512,128]{2,1,0:T(8,128)(2,1)S(1)} all-to-all(bf16[8,512,128]{2,1,0:T(8,128)(2,1)S(1)} %get-tuple-element.5), channel_id=1, replica_groups=mesh['fs'=8,'tp'=4] {'fs'}, dimensions={0} | all-to-all | bytes 2097152 | tf_op jit(solution)/shard_map/all_to_all | solution.py:39
  137.1 3.6 %all-to-all-start.1 = ((bf16[8,512,128]{2,1,0:T(8,128)(2,1)}), bf16[8,512,128]{2,1,0:T(8,128)(2,1)S(1)}, u32[]{:S(2)}, u32[]{:S(2)}) async-start(bf16[8,512,128]{2,1,0:T(8,128)(2,1)} %get-tuple-element.4), calls=%async_computation.1 | async-start | bytes 2097152 | tf_op jit(solution)/shard_map/all_to_all | solution.py:40
  140.7 2.7 convert_element_type.40
  143.4 41.7 %all-gather.3.cloned.1.call-done = bf16[1536,4096]{1,0:T(8,128)(2,1)} async-done(((bf16[1536,1024]{1,0:T(8,128)(2,1)}), bf16[1536,4096]{1,0:T(8,128)(2,1)}) %all-gather.3.cloned.1.call-update) | async-done | bytes 12582928 | tf_op jit(solution)/shard_map/all_gather | solution.py:57
  185.1 6.4 %fusion.11 = f32[1536,128]{1,0:T(8,128)S(1)} fusion(bf16[1536,4096]{1,0:T(8,128)(2,1)} %all-gather.3.cloned.1.call-done, bf16[4096,128]{1,0:T(8,128)(2,1)S(1)} %bitcast.33), kind=kOutput, calls=%fused_computation.38 | convolution fusion | flops 1610612736 | bytes 14417920 | tf_op jit(solution)/shard_map/dot_general | solution.py:58
  191.5 5.5 %all-to-all-start.2 = ((bf16[8,512,128]{2,1,0:T(8,128)(2,1)}), bf16[8,512,128]{2,1,0:T(8,128)(2,1)S(1)}, u32[]{:S(2)}, u32[]{:S(2)}) async-start(bf16[8,512,128]{2,1,0:T(8,128)(2,1)} %convert_element_type.40), calls=%async_computation.2 | async-start | bytes 2097152 | tf_op jit(solution)/shard_map/all_to_all | solution.py:41
  197.1 7.4 %fusion = bf16[1536,128]{1,0:T(8,128)(2,1)} fusion(bf16[1536,4096]{1,0:T(8,128)(2,1)} %all-gather.3.cloned.1.call-done, bf16[4096,128]{1,0:T(8,128)(2,1)S(1)} %bitcast.35, f32[1536,128]{1,0:T(8,128)S(1)} %fusion.11), kind=kOutput, calls=%fused_computation.7 | convolution fusion | flops 1611792384 | bytes 14811136 | tf_op jit(solution)/shard_map/dot_general | solution.py:59
  204.5 18.7 %all-to-all-done.2 = bf16[8,512,128]{2,1,0:T(8,128)(2,1)S(1)} async-done(((bf16[8,512,128]{2,1,0:T(8,128)(2,1)}), bf16[8,512,128]{2,1,0:T(8,128)(2,1)S(1)}, u32[]{:S(2)}, u32[]{:S(2)}) %all-to-all-start.2) | async-done | bytes 1048608 | tf_op jit(solution)/shard_map/all_to_all | solution.py:41
  223.3 16.8 %all_to_all.67 = bf16[4,1024,128]{2,1,0:T(8,128)(2,1)S(1)} all-to-all(bf16[4,1024,128]{2,1,0:T(8,128)(2,1)S(1)} %bitcast.31), channel_id=1, replica_groups=mesh['fs'=8,'tp'=4] {'tp'}, dimensions={0} | all-to-all | bytes 2097152 | tf_op jit(solution)/shard_map/all_to_all | solution.py:62
  240.7 4.9 %convolution_convert_fusion = bf16[1536,1024]{1,0:T(8,128)(2,1)} fusion(bf16[1536,512]{1,0:T(8,128)(2,1)} %all-gather.5.cloned.1.call-done, bf16[1024,512]{0,1:T(8,128)(2,1)S(1)} %bitcast.39), kind=kOutput, calls=%fused_computation.4 | convolution fusion | flops 1612185600 | bytes 5767168 | tf_op jit(solution)/shard_map/dot_general | solution.py:63
  245.5 4.0 %all-to-all-start.5 = ((bf16[8,192,1024]{2,1,0:T(8,128)(2,1)}), bf16[8,192,1024]{2,1,0:T(8,128)(2,1)S(1)}, u32[]{:S(2)}, u32[]{:S(2)}) async-start(bf16[8,192,1024]{2,1,0:T(8,128)(2,1)} %bitcast.38), calls=%async_computation.5 | async-start | bytes 6291456 | tf_op jit(solution)/shard_map/all_to_all | solution.py:67
  250.1 69.8 %all-to-all-done.5 = bf16[8,192,1024]{2,1,0:T(8,128)(2,1)S(1)} async-done(((bf16[8,192,1024]{2,1,0:T(8,128)(2,1)}), bf16[8,192,1024]{2,1,0:T(8,128)(2,1)S(1)}, u32[]{:S(2)}, u32[]{:S(2)}) %all-to-all-start.5) | async-done | bytes 3145760 | tf_op jit(solution)/shard_map/all_to_all | solution.py:67
  319.9 3.6 %gather_fusion.1 = bf16[768,1024]{1,0:T(8,128)(2,1)} fusion(bf16[1536,1024]{1,0:T(8,128)(2,1)S(1)} %bitcast.28, s32[1024]{0:T(1024)S(1)} %pad_clamp_fusion.1), kind=kCustom, calls=%fused_computation.1 | custom fusion | bytes 3148800 | tf_op jit(solution)/shard_map/gather | solution.py:71
  323.4 3.4 reshape.138
  326.9 4.8 %multiply_reduce_fusion = bf16[384,1024]{1,0:T(8,128)(2,1)} fusion(f32[384,2,1024]{2,1,0:T(2,128)S(1)} %reshape.138, f32[384,2]{1,0:T(8,128)S(1)} %copy.27), kind=kLoop, calls=%fused_computation.5 | loop fusion | flops 1179648 | bytes 3935232 | tf_op jit(solution)/shard_map/reduce_sum | solution.py:72
  331.7 1.0 copy.37
  (51 shorter events, 5.6 us)
Async XLA Ops:
  7.2 177.9 %all-gather.3.cloned.1.call-start = ((), (), s32[]{:S(2)}) async-start(), calls=%async_computation.6 | async-start | bytes 15728640 | tf_op jit(solution)/shard_map/all_gather | solution.py:57
  103.8 1.6 copy-start.6
  103.8 1.6 copy-start.9
  137.1 54.4 %copy-start.2 = (bf16[8,512,128]{2,1,0:T(8,128)(2,1)}, bf16[8,512,128]{2,1,0:T(8,128)(2,1)S(1)}, u32[]{:S(2)}) copy-start(bf16[8,512,128]{2,1,0:T(8,128)(2,1)S(1)} %all_to_all.66) | copy-start | bytes 3145732
  137.1 54.4 %all-to-all-start.1 = ((bf16[8,512,128]{2,1,0:T(8,128)(2,1)}), bf16[8,512,128]{2,1,0:T(8,128)(2,1)S(1)}, u32[]{:S(2)}, u32[]{:S(2)}) async-start(bf16[8,512,128]{2,1,0:T(8,128)(2,1)} %get-tuple-element.4), calls=%async_computation.1 | async-start | bytes 2097152 | tf_op jit(solution)/shard_map/all_to_all | solution.py:40
  191.5 13.0 %copy-start.4 = (bf16[8,512,128]{2,1,0:T(8,128)(2,1)}, bf16[8,512,128]{2,1,0:T(8,128)(2,1)S(1)}, u32[]{:S(2)}) copy-start(bf16[8,512,128]{2,1,0:T(8,128)(2,1)S(1)} %all-to-all-done.1) | copy-start | bytes 3145732
  191.5 31.7 %all-to-all-start.2 = ((bf16[8,512,128]{2,1,0:T(8,128)(2,1)}), bf16[8,512,128]{2,1,0:T(8,128)(2,1)S(1)}, u32[]{:S(2)}, u32[]{:S(2)}) async-start(bf16[8,512,128]{2,1,0:T(8,128)(2,1)} %convert_element_type.40), calls=%async_computation.2 | async-start | bytes 2097152 | tf_op jit(solution)/shard_map/all_to_all | solution.py:41
  197.1 43.6 %all-gather.5.cloned.1.call-start = ((), (), s32[]{:S(2)}) async-start(), calls=%async_computation.7 | async-start | bytes 1966080 | tf_op jit(solution)/shard_map/all_gather | solution.py:61
  223.3 22.3 %copy-start = (bf16[8,512,128]{2,1,0:T(8,128)(2,1)}, bf16[8,512,128]{2,1,0:T(8,128)(2,1)S(1)}, u32[]{:S(2)}) copy-start(bf16[8,512,128]{2,1,0:T(8,128)(2,1)S(1)} %all-to-all-done.2) | copy-start | bytes 3145732
  245.5 4.0 %copy-start.8 = (s32[384,2]{0,1:T(2,128)S(1)}, s32[384,2]{0,1:T(2,128)}, u32[]{:S(2)}) copy-start(s32[384,2]{0,1:T(2,128)} %param.12) | copy-start | bytes 9220
  245.5 4.3 %copy-start.7 = (f32[384,2]{0,1:T(2,128)S(1)}, f32[384,2]{0,1:T(2,128)}, u32[]{:S(2)}) copy-start(f32[384,2]{0,1:T(2,128)} %param.13) | copy-start | bytes 9220
  245.5 74.3 %all-to-all-start.5 = ((bf16[8,192,1024]{2,1,0:T(8,128)(2,1)}), bf16[8,192,1024]{2,1,0:T(8,128)(2,1)S(1)}, u32[]{:S(2)}, u32[]{:S(2)}) async-start(bf16[8,192,1024]{2,1,0:T(8,128)(2,1)} %bitcast.38), calls=%async_computation.5 | async-start | bytes 6291456 | tf_op jit(solution)/shard_map/all_to_all | solution.py:67
  326.8 4.8 %copy-start.3 = (bf16[8,512,128]{2,1,0:T(8,128)(2,1)S(1)}, bf16[8,512,128]{2,1,0:T(8,128)(2,1)}, u32[]{:S(2)}) copy-start(bf16[8,512,128]{2,1,0:T(8,128)(2,1)} %copy-done.2) | copy-start | bytes 3145732
  326.9 5.8 %copy-start.5 = (bf16[8,512,128]{2,1,0:T(8,128)(2,1)S(1)}, bf16[8,512,128]{2,1,0:T(8,128)(2,1)}, u32[]{:S(2)}) copy-start(bf16[8,512,128]{2,1,0:T(8,128)(2,1)} %copy-done.4) | copy-start | bytes 3145732
  326.9 6.8 %copy-start.1 = (bf16[8,512,128]{2,1,0:T(8,128)(2,1)S(1)}, bf16[8,512,128]{2,1,0:T(8,128)(2,1)}, u32[]{:S(2)}) copy-start(bf16[8,512,128]{2,1,0:T(8,128)(2,1)} %copy-done) | copy-start | bytes 3145732
Sparse Core Ops, SparseCore 0:
  103.9 81.1 all-gather.2
  204.6 20.2 all-gather.4
where the time goes:
time: 342 us; the launch traced here: 341 us
  waiting for transfers between devices  130 us (38%)
  blocking collectives  129 us (38%)
  local copies, waits for them, and re-layouts  19.7 us (6%)
  matrix products  18.6 us (5%)
  other arithmetic  16 us (5%)
  between operations  14.3 us (4%)
  starting transfers between devices  13.1 us (4%)
    all_to_all x1, blocking collectives, body(): lax.all_to_all(outgoing, 'fs', split_axis=0, concat_axis=0, tiled=True)  75.4 us
    all_to_all x1, waiting for transfers between devices, body(): lax.all_to_all(summed.reshape(-1, capacity, summed.shape[1]), 'fs', split...  69.8 us
    all_gather x1, waiting for transfers between devices, body(): segment = lax.all_gather(arrived, 'tp', axis=1, tiled=True)  41.7 us
    all_to_all x1, blocking collectives, body(): lax.all_to_all(gate_cast, 'fs', split_axis=0, concat_axis=1, tiled=True)  28.8 us
    all_to_all x1, waiting for transfers between devices, body(): lax.all_to_all(down_cast, 'fs', split_axis=0, concat_axis=1, tiled=True)  18.7 us
    all_to_all x1, blocking collectives, body(): lax.all_to_all(down_out[0], 'tp', split_axis=0, concat_axis=1, tiled=True)  16.8 us
    psum x1, blocking collectives, body(): sumsquares = lax.psum(jnp.sum(token_float * token_float, axis=1), 'tp')  8.39 us
    dot_general x1, matrix products, body(): up_val = jnp.dot(segment, up_mat, preferred_element_type=jnp.float32)  7.37 us
  transfers between devices with their start and end apart: 5, of which 3 were waited for; matrix products, arithmetic and copies ran while one was open for 6% of the time, Pallas kernels for 0%

commit v1 on v0

v1 whole, which is shorter than its diff:
```python
import jax
import jax.numpy as jnp
from jax import lax
from jax.sharding import PartitionSpec as P

norm_eps = 1e-06


def half_shift(step, size):
    half = size // 2
    return [(s, s // half * half + (s % half + step) % half) for s in range(size)]


def cross_swap(size):
    return [(s, (s + size // 2) % size) for s in range(size)]


def body(tokens, gate_master, up_master, down_master, norm_gain, routes, route_weight):
    n_experts = gate_master.shape[0]
    tok_rows, top_count = routes.shape
    capacity = 2 * tok_rows * top_count // n_experts
    n_tp = lax.axis_size("tp")
    n_fs = lax.axis_size("fs")
    half = n_tp // 2
    width = tokens.shape[1]
    hidden_cols = gate_master.shape[2]
    me_fs = lax.axis_index("fs")
    me_tp = lax.axis_index("tp")

    all_rows = lax.all_gather(tokens, "fs", axis=0)

    folded = norm_gain[None, :, None]
    gate_cast = (gate_master * folded).astype(jnp.bfloat16)
    up_cast = (up_master * folded).astype(jnp.bfloat16)
    down_cast = down_master.astype(jnp.bfloat16)
    gate_out = lax.all_to_all(gate_cast, "fs", split_axis=0, concat_axis=1, tiled=True)
    up_out = lax.all_to_all(up_cast, "fs", split_axis=0, concat_axis=1, tiled=True)
    down_out = lax.all_to_all(down_cast, "fs", split_axis=0, concat_axis=1, tiled=True)

    token_float = tokens.astype(jnp.float32)
    sumsquares = lax.psum(jnp.sum(token_float * token_float, axis=1), "tp")
    inverse = lax.rsqrt(sumsquares / (width * n_tp) + norm_eps)
    mix = route_weight / jnp.sum(route_weight, axis=1, keepdims=True)
    facts = jnp.concatenate([inverse[None], routes.T.astype(jnp.float32), mix.T], axis=0)
    facts = lax.all_gather(facts, "fs", axis=0)
    inverse_all = facts[:, 0]
    named = facts[:, 1 : 1 + top_count] == me_fs.astype(jnp.float32)
    hit = jnp.any(named, axis=1)
    mix_all = jnp.sum(jnp.where(named, facts[:, 1 + top_count :], 0.0), axis=1)
    earlier = jnp.arange(tok_rows)[:, None] < jnp.arange(tok_rows)[None, :]
    slot = jnp.dot(
        hit.astype(jnp.bfloat16), earlier.astype(jnp.bfloat16), preferred_element_type=jnp.float32
    ).astype(jnp.int32)
    place = jnp.where(hit, slot, -1)
    match = place[:, None, :] == jnp.arange(capacity, dtype=jnp.int32)[None, :, None]
    inverse_slot = jnp.sum(jnp.where(match, inverse_all[:, None, :], 0.0), axis=2)
    mix_slot = jnp.sum(jnp.where(match, mix_all[:, None, :], 0.0), axis=2)
    onehot = match.astype(jnp.bfloat16)

    rows = lax.dot_general(
        onehot, all_rows, (((2,), (1,)), ((0,), (0,))), preferred_element_type=jnp.float32
    )
    rows = (rows * inverse_slot[:, :, None]).astype(jnp.bfloat16).reshape(-1, width)

    my_half = me_tp // half
    inside = me_tp % half
    span = half * width
    keep = my_half * span
    give = (1 - my_half) * span

    def rows_of(start):
        return jnp.concatenate(
            [lax.dynamic_slice_in_dim(w[0], start, span, 0) for w in (gate_out, up_out)], axis=1
        )

    own_cols = rows_of(keep)
    partner_cols = lax.ppermute(rows_of(give), "tp", cross_swap(n_tp))

    pieces = [rows] + [lax.ppermute(rows, "tp", half_shift(j, n_tp)) for j in range(1, half)]

    def partial(cols):
        total = 0.0
        for j, piece in enumerate(pieces):
            start = ((inside + half - j) % half) * width
            block = lax.dynamic_slice_in_dim(cols, start, width, 0)
            total = total + jnp.dot(piece, block, preferred_element_type=jnp.float32)
        return total

    for_partner = lax.ppermute(partial(partner_cols).astype(jnp.bfloat16), "tp", cross_swap(n_tp))
    both = partial(own_cols) + for_partner.astype(jnp.float32)
    hidden = (jax.nn.silu(both[:, :hidden_cols]) * both[:, hidden_cols:]).astype(jnp.bfloat16)
    hidden_whole = lax.all_gather(hidden, "tp", axis=1, tiled=True)
    down_quarter = lax.all_to_all(down_out[0], "tp", split_axis=0, concat_axis=1, tiled=True)
    result = lax.dot_general(
        hidden_whole, down_quarter, (((1,), (1,)), ((), ())), preferred_element_type=jnp.float32
    )
    weighted = (result * mix_slot.reshape(-1, 1)).astype(jnp.bfloat16)
    spread = lax.dot_general(
        onehot,
        weighted.reshape(n_fs, capacity, -1),
        (((1,), (1,)), ((0,), (0,))),
        preferred_element_type=jnp.float32,
    ).astype(jnp.bfloat16)
    mixed = lax.psum_scatter(
        spread.reshape(n_fs * tok_rows, -1), "fs", scatter_dimension=0, tiled=True
    )
    return (gate_out, up_out, down_out, mixed)


def solution(mesh):
    placed = (
        P("fs", "tp"),
        P(None, "fs", "tp"),
        P(None, "fs", "tp"),
        P(None, "fs", "tp"),
        P("fs"),
        P("fs", None),
        P("fs", None),
    )
    return jax.shard_map(
        body,
        mesh=mesh,
        in_specs=placed,
        out_specs=(P("fs", None, "tp"), P("fs", None, "tp"), P("fs", None, "tp"), P("fs", "tp")),
        check_vma=False,
    )
```

time: 342 us -> 385 us (1.13)
  waiting for transfers between devices: 130 us -> 235 us
  blocking collectives: 129 us -> 70.2 us
  starting transfers between devices: 13.1 us -> 22.8 us
  local copies, waits for them, and re-layouts: 19.7 us -> 10.5 us
  other arithmetic: 16 us -> 8.56 us
  matrix products: 18.6 us -> 23.8 us
    all_to_all x3 -> x0, blocking collectives: 121 us -> none  [the longest x1 75.4 us: body(): lax.all_to_all(outgoing, 'fs', split_axis=0, concat_axis=0, tiled=True)]
    reduce_scatter x0 -> x1, waiting for transfers between devices: none -> 118 us  [body(): lax.psum_scatter(spread.reshape(n_fs * tok_rows, -1), 'fs', scatter_dimen...]
    all_gather x0 -> x1, blocking collectives: none -> 63.6 us  [body(): facts = lax.all_gather(facts, 'fs', axis=0)]
    all_to_all x1 -> x2, waiting for transfers between devices: 69.8 us -> 15.5 us  [the longest x1 15.5 us: body(): lax.all_to_all(down_out[0], 'tp', split_axis=0, concat_axis=1, tiled=True)]
    ppermute x0 -> x3, waiting for transfers between devices: none -> 34.6 us  [the longest x1 24.3 us: body(): partner_cols = lax.ppermute(rows_of(give), 'tp', cross_swap(n_tp))]
    all_gather x1, waiting for transfers between devices: 41.7 us -> 56.9 us  [body(): all_rows = lax.all_gather(tokens, 'fs', axis=0)]
    all_to_all x1, waiting for transfers between devices: 18.7 us -> 9 us  [body(): lax.all_to_all(down_cast, 'fs', split_axis=0, concat_axis=1, tiled=True)]
    gather x2 -> x0, local copies, waits for them, and re-layouts: 9.4 us -> none  [the longest x1 5.84 us: place_rows(): return padded[chosen]]
  transfers between devices with their start and end apart: 5 -> 10, of which waited for: 3 -> 6; matrix products, arithmetic and copies ran while one was open for 6% -> 6% of each run, Pallas kernels for 0% -> 0%
where the time goes in v1:
time: 385 us
  waiting for transfers between devices  235 us (61%)
  blocking collectives  70.2 us (18%)
  matrix products  23.8 us (6%)
  starting transfers between devices  22.8 us (6%)
  between operations  14 us (4%)
  local copies, waits for them, and re-layouts  10.5 us (3%)
  other arithmetic  8.56 us (2%)
    reduce_scatter x1, waiting for transfers between devices, body(): lax.psum_scatter(spread.reshape(n_fs * tok_rows, -1), 'fs', scatter_dimen...  118 us
    all_gather x1, blocking collectives, body(): facts = lax.all_gather(facts, 'fs', axis=0)  63.6 us
    all_gather x1, waiting for transfers between devices, body(): all_rows = lax.all_gather(tokens, 'fs', axis=0)  56.9 us
    ppermute x1, waiting for transfers between devices, body(): partner_cols = lax.ppermute(rows_of(give), 'tp', cross_swap(n_tp))  24.3 us
    all_to_all x1, waiting for transfers between devices, body(): lax.all_to_all(down_out[0], 'tp', split_axis=0, concat_axis=1, tiled=True)  15.5 us
    dot_general x4, matrix products, partial(): total = total + jnp.dot(piece, block, preferred_element_type=jnp.float32)  11.3 us
    ppermute x1, waiting for transfers between devices, body(): lax.ppermute(partial(partner_cols).astype(jnp.bfloat16), 'tp', cross_swap...  10.3 us
    all_to_all x1, waiting for transfers between devices, body(): lax.all_to_all(down_cast, 'fs', split_axis=0, concat_axis=1, tiled=True)  9 us
  transfers between devices with their start and end apart: 10, of which 6 were waited for; matrix products, arithmetic and copies ran while one was open for 6% of the time, Pallas kernels for 0%

profile of v1, /device:TPU:0, one launch (start us, length us, event | category | flops | bytes accessed | tf_op | source)
XLA Modules:
  0.0 384.8 jit_solution(12529231379481492038)
XLA Ops:
  7.9 4.1 %multiply_convert_fusion.2 = (bf16[8,512,128]{2,1,0:T(8,128)(2,1)}, bf16[8,512,128]{2,1,0:T(8,128)(2,1)}) fusion(f32[8,512,128]{2,1,0:T(8,128)} %param.9, f32[512]{0:T(512)} %param.11, f32[8,512,128]{2,1,0:T(8,128)} %param.8), kind=kLoop, calls=%fused_computation.10 | loop fusion | flops 2097152 | bytes 6293504 | tf_op jit(solution)/shard_map/convert_element_type | solution.py:34
  12.0 7.4 %all-to-all-start = ((bf16[8,512,128]{2,1,0:T(8,128)(2,1)}), bf16[8,512,128]{2,1,0:T(8,128)(2,1)S(1)}, u32[]{:S(2)}, u32[]{:S(2)}) async-start(bf16[8,512,128]{2,1,0:T(8,128)(2,1)} %get-tuple-element.11), calls=%async_computation | async-start | bytes 2097152 | tf_op jit(solution)/shard_map/all_to_all | solution.py:36
  19.7 6.6 %psum.7 = f32[384]{0:T(512)S(1)} all-reduce(f32[384]{0:T(512)S(1)} %multiply_reduce_fusion), channel_id=1, replica_groups=mesh['fs'=8,'tp'=4] {'tp'}, use_global_device_ids=true, to_apply=%region_1.0 | all-reduce | flops 384 | bytes 3072 | tf_op jit(solution)/shard_map/psum | solution.py:41
  26.4 63.6 %all-gather.2 = f32[8,5,384]{2,1,0:T(8,128)S(1)} all-gather(f32[1,5,384]{2,1,0:T(8,128)S(1)} %maximum_bitcast_fusion), channel_id=2, replica_groups=mesh['fs'=8,'tp'=4] {'fs'}, dimensions={0}, use_global_device_ids=true | all-gather | bytes 69120 | tf_op jit(solution)/shard_map/all_gather | solution.py:45
  91.1 4.3 %all-to-all-start.1 = ((bf16[8,512,128]{2,1,0:T(8,128)(2,1)}), bf16[8,512,128]{2,1,0:T(8,128)(2,1)}, u32[]{:S(2)}, u32[]{:S(2)}) async-start(bf16[8,512,128]{2,1,0:T(8,128)(2,1)} %get-tuple-element.10), calls=%async_computation.1 | async-start | bytes 2097152 | tf_op jit(solution)/shard_map/all_to_all | solution.py:37
  95.4 56.9 %all-gather.8.cloned.1.call-done = bf16[3072,1024]{1,0:T(8,128)(2,1)} async-done(((bf16[384,1024]{1,0:T(8,128)(2,1)}), bf16[3072,1024]{1,0:T(8,128)(2,1)}) %all-gather.8.cloned.1.call-update) | async-done | bytes 6291472 | tf_op jit(solution)/shard_map/all_gather | solution.py:30
  152.3 4.6 %multiply_convert_fusion.1 = bf16[8,192,1024]{2,1,0:T(8,128)(2,1)S(1)} fusion(f32[8,192]{1,0:T(8,128)S(1)} %get-tuple-element.5, bf16[8,384,1024]{2,1,0:T(8,128)(2,1)} %bitcast.31, s32[8,384]{1,0:T(8,128)S(1)} %fusion.4), kind=kOutput, calls=%fused_computation.1 | convolution fusion | flops 1211695104 | bytes 9455616 | tf_op jit(solution)/shard_map/dot_general | solution.py:60
  157.0 2.2 constant_dynamic-slice_fusion.1
  159.3 2.1 constant_dynamic-slice_fusion
  164.0 24.3 %collective-permute-done.1 = bf16[2048,256]{1,0:T(8,128)(2,1)} collective-permute-done((bf16[2048,256]{1,0:T(8,128)(2,1)}, bf16[2048,256]{1,0:T(8,128)(2,1)}, u32[]{:S(2)}, u32[]{:S(2)}) %collective-permute-start.1) | collective-permute-done | bytes 1048608 | tf_op jit(solution)/shard_map/ppermute | solution.py:77
  188.4 3.0 fusion.11
  191.4 3.1 fusion.1
  197.1 4.2 %all-to-all-start.2 = ((bf16[8,512,128]{2,1,0:T(8,128)(2,1)}), bf16[8,512,128]{2,1,0:T(8,128)(2,1)}, u32[]{:S(2)}, u32[]{:S(2)}) async-start(bf16[8,512,128]{2,1,0:T(8,128)(2,1)} %convert_element_type.47), calls=%async_computation.2 | async-start | bytes 2097152 | tf_op jit(solution)/shard_map/all_to_all | solution.py:38
  201.4 2.1 fusion.9
  203.5 10.3 %collective-permute-done.2 = bf16[1536,256]{1,0:T(8,128)(2,1)} collective-permute-done((bf16[1536,256]{1,0:T(8,128)(2,1)}, bf16[1536,256]{1,0:T(8,128)(2,1)}, u32[]{:S(2)}, u32[]{:S(2)}) %collective-permute-start.2) | collective-permute-done | bytes 786464 | tf_op jit(solution)/shard_map/ppermute | solution.py:89
  213.8 3.1 fusion
  217.9 9.0 %all-to-all-done.2 = bf16[8,512,128]{2,1,0:T(8,128)(2,1)} async-done(((bf16[8,512,128]{2,1,0:T(8,128)(2,1)}), bf16[8,512,128]{2,1,0:T(8,128)(2,1)}, u32[]{:S(2)}, u32[]{:S(2)}) %all-to-all-start.2) | async-done | bytes 1048608 | tf_op jit(solution)/shard_map/all_to_all | solution.py:38
  226.9 3.5 all-to-all-start.3
  230.8 15.5 %all-to-all-done.3 = bf16[4,1024,128]{2,1,0:T(8,128)(2,1)S(1)} async-done(((bf16[4,1024,128]{2,1,0:T(8,128)(2,1)}), bf16[4,1024,128]{2,1,0:T(8,128)(2,1)S(1)}, u32[]{:S(2)}, u32[]{:S(2)}) %all-to-all-start.3) | async-done | bytes 1048608 | tf_op jit(solution)/shard_map/all_to_all | solution.py:93
  246.9 3.2 multiply_convert_fusion
  250.1 4.5 %convolution_convert_fusion = bf16[8,384,1024]{2,1,0:T(8,128)(2,1)} fusion(bf16[8,192,1024]{2,1,0:T(8,128)(2,1)S(1)} %bitcast.38, s32[8,384]{1,0:T(8,128)S(1)} %fusion.4), kind=kOutput, calls=%fused_computation.2 | convolution fusion | flops 1211695104 | bytes 9449472 | tf_op jit(solution)/shard_map/dot_general | solution.py:98
  254.7 118.2 %reduce-scatter.2.cloned.1.call-done = bf16[384,1024]{1,0:T(8,128)(2,1)} async-done(((bf16[3072,1024]{1,0:T(8,128)(2,1)}), bf16[384,1024]{1,0:T(8,128)(2,1)}) %reduce-scatter.2.cloned.1.call-update) | async-done | bytes 786448 | tf_op jit(solution)/shard_map/reduce_scatter | solution.py:104
  373.8 2.3 copy.20
  376.1 2.3 copy.21
  (50 shorter events, 10.3 us)
Async XLA Ops:
  7.2 145.2 %all-gather.8.cloned.1.call-start = ((), (), s32[]{:S(2)}) async-start(), calls=%async_computation.7 | async-start | bytes 7077888 | tf_op jit(solution)/shard_map/all_gather | solution.py:30
  12.0 7.4 %copy-start.2 = (bf16[384,1024]{1,0:T(8,128)(2,1)S(1)}, bf16[384,1024]{1,0:T(8,128)(2,1)}, u32[]{:S(2)}) copy-start(bf16[384,1024]{1,0:T(8,128)(2,1)} %param.7) | copy-start | bytes 2359300
  12.0 14.3 %copy-start.7 = (f32[384,2]{0,1:T(2,128)S(1)}, f32[384,2]{0,1:T(2,128)}, u32[]{:S(2)}) copy-start(f32[384,2]{0,1:T(2,128)} %param.13) | copy-start | bytes 9220
  12.0 14.3 %copy-start.8 = (s32[384,2]{0,1:T(2,128)S(1)}, s32[384,2]{0,1:T(2,128)}, u32[]{:S(2)}) copy-start(s32[384,2]{0,1:T(2,128)} %param.12) | copy-start | bytes 9220
  12.0 79.1 %all-to-all-start = ((bf16[8,512,128]{2,1,0:T(8,128)(2,1)}), bf16[8,512,128]{2,1,0:T(8,128)(2,1)S(1)}, u32[]{:S(2)}, u32[]{:S(2)}) async-start(bf16[8,512,128]{2,1,0:T(8,128)(2,1)} %get-tuple-element.11), calls=%async_computation | async-start | bytes 2097152 | tf_op jit(solution)/shard_map/all_to_all | solution.py:36
  91.1 61.2 %copy-start = (bf16[8,512,128]{2,1,0:T(8,128)(2,1)}, bf16[8,512,128]{2,1,0:T(8,128)(2,1)S(1)}, u32[]{:S(2)}) copy-start(bf16[8,512,128]{2,1,0:T(8,128)(2,1)S(1)} %all-to-all-done) | copy-start | bytes 3145732
  91.1 68.2 %all-to-all-start.1 = ((bf16[8,512,128]{2,1,0:T(8,128)(2,1)}), bf16[8,512,128]{2,1,0:T(8,128)(2,1)}, u32[]{:S(2)}, u32[]{:S(2)}) async-start(bf16[8,512,128]{2,1,0:T(8,128)(2,1)} %get-tuple-element.10), calls=%async_computation.1 | async-start | bytes 2097152 | tf_op jit(solution)/shard_map/all_to_all | solution.py:37
  156.9 31.4 %collective-permute-start = (bf16[1536,1024]{1,0:T(8,128)(2,1)S(1)}, bf16[1536,1024]{1,0:T(8,128)(2,1)}, u32[]{:S(2)}, u32[]{:S(2)}) collective-permute-start(bf16[1536,1024]{1,0:T(8,128)(2,1)S(1)} %bitcast.32), channel_id=1, source_target_pairs={{0,1},{1,0},{2,3},{3,2},{4,5},{5,4},{6,7},{7,6},{8,9},{9,8},{10,11... | collective-permute-start | bytes 9437192 | tf_op jit(solution)/shard_map/ppermute | solution.py:79
  159.3 2.1 copy-start.6
  162.5 25.8 %collective-permute-start.1 = (bf16[2048,256]{1,0:T(8,128)(2,1)}, bf16[2048,256]{1,0:T(8,128)(2,1)}, u32[]{:S(2)}, u32[]{:S(2)}) collective-permute-start(bf16[2048,256]{1,0:T(8,128)(2,1)} %pad_maximum_fusion), channel_id=1, source_target_pairs={{0,2},{1,3},{2,0},{3,1},{4,6},{5,7},{6,4},{7,5},{8,10},{9,11},{10,... | collective-permute-start | bytes 3145736 | tf_op jit(solution)/shard_map/ppermute | solution.py:77
  191.4 4.6 %copy-start.3 = (f32[8,512,128]{2,1,0:T(8,128)S(1)}, f32[8,512,128]{2,1,0:T(8,128)}, u32[]{:S(2)}) copy-start(f32[8,512,128]{2,1,0:T(8,128)} %param.10) | copy-start | bytes 6291460
  194.4 19.4 %collective-permute-start.2 = (bf16[1536,256]{1,0:T(8,128)(2,1)}, bf16[1536,256]{1,0:T(8,128)(2,1)}, u32[]{:S(2)}, u32[]{:S(2)}) collective-permute-start(bf16[1536,256]{1,0:T(8,128)(2,1)} %fusion.1), channel_id=1, source_target_pairs={{0,2},{1,3},{2,0},{3,1},{4,6},{5,7},{6,4},{7,5},{8,10},{9,11},{10,... | collective-permute-start | bytes 2359304 | tf_op jit(solution)/shard_map/ppermute | solution.py:89
  197.1 29.8 %all-to-all-start.2 = ((bf16[8,512,128]{2,1,0:T(8,128)(2,1)}), bf16[8,512,128]{2,1,0:T(8,128)(2,1)}, u32[]{:S(2)}, u32[]{:S(2)}) async-start(bf16[8,512,128]{2,1,0:T(8,128)(2,1)} %convert_element_type.47), calls=%async_computation.2 | async-start | bytes 2097152 | tf_op jit(solution)/shard_map/all_to_all | solution.py:38
  201.3 45.5 %all-gather.6.cloned.1.call-start = ((), (), s32[]{:S(2)}) async-start(), calls=%async_computation.5 | async-start | bytes 1966080 | tf_op jit(solution)/shard_map/all_gather | solution.py:92
  201.4 12.4 %copy-start.4 = (bf16[2048,128]{1,0:T(8,128)(2,1)S(1)}, bf16[2048,128]{1,0:T(8,128)(2,1)}, u32[]{:S(2)}) copy-start(bf16[2048,128]{1,0:T(8,128)(2,1)} %get-tuple-element.7) | copy-start | bytes 1572868
  201.4 12.4 %copy-start.5 = (bf16[2048,128]{1,0:T(8,128)(2,1)S(1)}, bf16[2048,128]{1,0:T(8,128)(2,1)}, u32[]{:S(2)}) copy-start(bf16[2048,128]{1,0:T(8,128)(2,1)} %get-tuple-element.9) | copy-start | bytes 1572868
  226.9 19.4 %all-to-all-start.3 = ((bf16[4,1024,128]{2,1,0:T(8,128)(2,1)}), bf16[4,1024,128]{2,1,0:T(8,128)(2,1)S(1)}, u32[]{:S(2)}, u32[]{:S(2)}) async-start(bf16[4,1024,128]{2,1,0:T(8,128)(2,1)} %bitcast.10), calls=%async_computation.3 | async-start | bytes 2097152 | tf_op jit(solution)/shard_map/all_to_all | solution.py:93
  230.5 142.4 %reduce-scatter.2.cloned.1.call-start = ((), (), s32[]{:S(2)}) async-start(), calls=%async_computation.6 | async-start | bytes 7077888 | tf_op jit(solution)/shard_map/reduce_scatter | solution.py:104
  254.6 118.2 %copy-start.1 = (bf16[8,512,128]{2,1,0:T(8,128)(2,1)S(1)}, bf16[8,512,128]{2,1,0:T(8,128)(2,1)}, u32[]{:S(2)}) copy-start(bf16[8,512,128]{2,1,0:T(8,128)(2,1)} %copy-done) | copy-start | bytes 3145732
Sparse Core Ops, SparseCore 0:
  10.2 142.1 all-gather.7
  218.1 20.1 all-gather.5
  254.8 117.9 reduce-scatter.1

commit v2 on v1

v2 whole, which is shorter than its diff:
```python
import jax
import jax.numpy as jnp
from jax import lax
from jax.sharding import PartitionSpec as P

norm_eps = 1e-06


def half_shift(step, size):
    half = size // 2
    return [(s, s // half * half + (s % half + step) % half) for s in range(size)]


def cross_swap(size):
    return [(s, (s + size // 2) % size) for s in range(size)]


def member_shift(step, crossed, size):
    half = size // 2
    return [
        (s, (s // half + crossed) % 2 * half + (s % half + step) % half) for s in range(size)
    ]


def body(tokens, gate_master, up_master, down_master, norm_gain, routes, route_weight):
    n_experts = gate_master.shape[0]
    tok_rows, top_count = routes.shape
    capacity = 2 * tok_rows * top_count // n_experts
    n_tp = lax.axis_size("tp")
    half = n_tp // 2
    width = tokens.shape[1]
    hidden_cols = gate_master.shape[2]
    me_tp = lax.axis_index("tp")
    chunks = 2 if capacity % 32 == 0 else 1
    part = capacity // chunks

    folded = norm_gain[None, :, None]
    pair = jnp.concatenate(
        [(gate_master * folded).astype(jnp.bfloat16), (up_master * folded).astype(jnp.bfloat16)], axis=2
    )
    pair = lax.all_to_all(pair, "fs", split_axis=0, concat_axis=1, tiled=True)
    down_cast, pair = lax.optimization_barrier((down_master.astype(jnp.bfloat16), pair))
    down_out = lax.all_to_all(down_cast, "fs", split_axis=0, concat_axis=1, tiled=True)
    gate_out = pair[:, :, :hidden_cols]
    up_out = pair[:, :, hidden_cols:]

    token_float = tokens.astype(jnp.float32)
    sumsquares = lax.psum(jnp.sum(token_float * token_float, axis=1), "tp")
    inverse = lax.rsqrt(sumsquares / (width * n_tp) + norm_eps)[:, None]
    normed = (token_float * inverse).astype(jnp.bfloat16)
    mix = route_weight / jnp.sum(route_weight, axis=1, keepdims=True)
    experts = jnp.arange(n_experts, dtype=jnp.int32)
    named = jnp.any(routes[:, :, None] == experts, axis=1)
    earlier = jnp.arange(tok_rows)[:, None] > jnp.arange(tok_rows)[None, :]
    before = jnp.dot(
        earlier.astype(jnp.bfloat16), named.astype(jnp.bfloat16), preferred_element_type=jnp.float32
    ).astype(jnp.int32)
    slots = jnp.sum(jnp.where(routes[:, :, None] == experts, before[:, None, :], 0), axis=2)
    place = (slots // part * n_experts + routes) * part + slots % part
    spots = jnp.arange(n_experts * capacity, dtype=jnp.int32)
    where_to = place[:, :, None] == spots
    onehot = jnp.any(where_to, axis=1).astype(jnp.bfloat16)
    mixing = jnp.sum(jnp.where(where_to, mix[:, :, None], 0.0), axis=1)
    mixing_high = mixing.astype(jnp.bfloat16)
    mixing_low = (mixing - mixing_high.astype(jnp.float32)).astype(jnp.bfloat16)
    outgoing = lax.dot_general(
        onehot, normed, (((0,), (0,)), ((), ())), preferred_element_type=jnp.float32
    ).astype(jnp.bfloat16)
    outgoing = outgoing.reshape(chunks, n_experts, part, width)

    my_half = me_tp // half
    inside = me_tp % half
    span = half * width
    own_cols = lax.dynamic_slice_in_dim(pair[0], my_half * span, span, 0)
    partner_cols = lax.ppermute(
        lax.dynamic_slice_in_dim(pair[0], (1 - my_half) * span, span, 0), "tp", cross_swap(n_tp)
    )

    arrived = []
    for c in range(chunks):
        if c == 0:
            ready, down_out, partner_cols = lax.optimization_barrier((outgoing[c], down_out, partner_cols))
        else:
            ready, arrived[-1] = lax.optimization_barrier((outgoing[c], last))
        last = lax.all_to_all(ready, "fs", split_axis=0, concat_axis=0, tiled=True)
        arrived.append(last)

    def in_order(cols):
        blocks = cols.reshape(half, width, cols.shape[1])
        return [
            lax.dynamic_index_in_dim(blocks, (inside + half - j) % half, 0, keepdims=False)
            for j in range(half)
        ]

    own_blocks, partner_blocks = in_order(own_cols), in_order(partner_cols)
    quarters = down_out[0].reshape(n_tp, -1, hidden_cols)
    picked = []
    for j in range(half):
        for crossed in range(2):
            target = (my_half + crossed) % 2 * half + (inside + j) % half
            piece = lax.dynamic_index_in_dim(quarters, target, 0, keepdims=False)
            if j + crossed > 0:
                piece = lax.ppermute(piece, "tp", member_shift(j, crossed, n_tp))
            picked.append(piece)
    down_mat = jnp.concatenate(picked, axis=1)

    def serve(rows):
        rows = rows.reshape(-1, width)
        pieces = [rows] + [lax.ppermute(rows, "tp", half_shift(j, n_tp)) for j in range(1, half)]

        def partial(blocks):
            total = 0.0
            for piece, block in zip(pieces, blocks):
                total = total + jnp.dot(piece, block, preferred_element_type=jnp.float32)
            return total

        swapped = lax.ppermute(partial(partner_blocks).astype(jnp.bfloat16), "tp", cross_swap(n_tp))
        both = partial(own_blocks) + swapped.astype(jnp.float32)
        hidden = (jax.nn.silu(both[:, :hidden_cols]) * both[:, hidden_cols:]).astype(jnp.bfloat16)
        two = jnp.concatenate([hidden, lax.ppermute(hidden, "tp", cross_swap(n_tp))], axis=1)
        all_hidden = [two] + [lax.ppermute(two, "tp", half_shift(j, n_tp)) for j in range(1, half)]
        result = lax.dot_general(
            jnp.concatenate(all_hidden, axis=1),
            down_mat,
            (((1,), (1,)), ((), ())),
            preferred_element_type=jnp.float32,
        )
        return result.astype(jnp.bfloat16).reshape(-1, part, width)

    returned = []
    for c in range(chunks):
        rows = arrived[c]
        if c > 0:
            rows, served = lax.optimization_barrier((rows, served))
            returned.append(lax.all_to_all(served, "fs", split_axis=0, concat_axis=0, tiled=True))
        served = serve(rows)
    returned.append(lax.all_to_all(served, "fs", split_axis=0, concat_axis=0, tiled=True))

    mixed = 0.0
    for c, back in enumerate(returned):
        flat = back.reshape(n_experts * part, width)
        for weights in (mixing_high, mixing_low):
            chosen = weights[:, c * n_experts * part : (c + 1) * n_experts * part]
            mixed = mixed + jnp.dot(chosen, flat, preferred_element_type=jnp.float32)
    return (gate_out, up_out, down_out, mixed.astype(jnp.bfloat16))


def solution(mesh):
    placed = (
        P("fs", "tp"),
        P(None, "fs", "tp"),
        P(None, "fs", "tp"),
        P(None, "fs", "tp"),
        P("fs"),
        P("fs", None),
        P("fs", None),
    )
    return jax.shard_map(
        body,
        mesh=mesh,
        in_specs=placed,
        out_specs=(P("fs", None, "tp"), P("fs", None, "tp"), P("fs", None, "tp"), P("fs", "tp")),
        check_vma=False,
    )
```

time: 385 us -> 271 us (0.70)
  waiting for transfers between devices: 235 us -> 134 us
  blocking collectives: 70.2 us -> 48.2 us
  between operations: 14 us -> 1.06 us
  starting transfers between devices: 22.8 us -> 35.2 us
  matrix products: 23.8 us -> 35.6 us
    reduce_scatter x1 -> x0, waiting for transfers between devices: 118 us -> none  [body(): lax.psum_scatter(spread.reshape(n_fs * tok_rows, -1), 'fs', scatter_dimen...]
    all_gather x1 -> x0, blocking collectives: 63.6 us -> none  [body(): facts = lax.all_gather(facts, 'fs', axis=0)]
    all_to_all x3 -> x4, waiting for transfers between devices: 15.6 us -> 75.6 us  [the longest x1 38.5 us: body(): pair = lax.all_to_all(pair, 'fs', split_axis=0, concat_axis=1, tiled=True)]
    all_gather x2 -> x0, waiting for transfers between devices: 57 us -> none  [the longest x1 56.9 us: body(): all_rows = lax.all_gather(tokens, 'fs', axis=0)]
    all_to_all x0 -> x1, blocking collectives: none -> 41.6 us  [body(): last = lax.all_to_all(ready, 'fs', split_axis=0, concat_axis=0, tiled=True)]
    ppermute x3 -> x12, waiting for transfers between devices: 34.6 us -> 58.1 us  [the longest x1 18.9 us: body(): lax.ppermute(lax.dynamic_slice_in_dim(pair[0], (1 - my_half) * span, span...]
    all_to_all x1, waiting for transfers between devices: 9 us -> 0.01 us  [body(): lax.all_to_all(down_cast, 'fs', split_axis=0, concat_axis=1, tiled=True)]
    ppermute x3 -> x12, starting transfers between devices: 3.08 us -> 10.2 us  [the longest x2 3.18 us: serve(): lax.ppermute(partial(partner_blocks).astype(jnp.bfloat16), 'tp', cross_sw...]
  transfers between devices with their start and end apart: 10 -> 17, of which waited for: 6 -> 11; matrix products, arithmetic and copies ran while one was open for 6% -> 15% of each run, Pallas kernels for 0% -> 0%
where the time goes in v2:
time: 271 us; the launch traced here: 270 us
  waiting for transfers between devices  134 us (49%)
  blocking collectives  48.2 us (18%)
  matrix products  35.6 us (13%)
  starting transfers between devices  35.2 us (13%)
  other arithmetic  9.17 us (3%)
  local copies, waits for them, and re-layouts  6.9 us (3%)
    all_to_all x1, blocking collectives, body(): last = lax.all_to_all(ready, 'fs', split_axis=0, concat_axis=0, tiled=True)  41.6 us
    all_to_all x1, waiting for transfers between devices, body(): pair = lax.all_to_all(pair, 'fs', split_axis=0, concat_axis=1, tiled=True)  38.5 us
    all_to_all x2, waiting for transfers between devices, body(): lax.all_to_all(served, 'fs', split_axis=0, concat_axis=0, tiled=True)  37 us
    ppermute x1, waiting for transfers between devices, body(): lax.ppermute(lax.dynamic_slice_in_dim(pair[0], (1 - my_half) * span, span...  18.9 us
    dot_general x8, matrix products, partial(): total = total + jnp.dot(piece, block, preferred_element_type=jnp.float32)  16.8 us
    ppermute x2, waiting for transfers between devices, serve(): lax.ppermute(partial(partner_blocks).astype(jnp.bfloat16), 'tp', cross_sw...  15.7 us
    dot_general x4, matrix products, body(): mixed = mixed + jnp.dot(chosen, flat, preferred_element_type=jnp.float32)  12.3 us
    ppermute x3, waiting for transfers between devices, body(): piece = lax.ppermute(piece, 'tp', member_shift(j, crossed, n_tp))  12.1 us
  transfers between devices with their start and end apart: 17, of which 11 were waited for; matrix products, arithmetic and copies ran while one was open for 15% of the time, Pallas kernels for 0%

profile of v2, /device:TPU:0, one launch (start us, length us, event | category | flops | bytes accessed | tf_op | source)
XLA Modules:
  0.0 269.9 jit_solution(13902517624220506767)
XLA Ops:
  0.6 2.8 %multiply_convert_fusion.1 = (bf16[8,512,128]{2,1,0:T(8,128)(2,1)S(1)}, bf16[8,512,128]{2,1,0:T(8,128)(2,1)S(1)}) fusion(f32[8,512,128]{2,1,0:T(8,128)} %param.8, f32[512]{0:T(512)} %param.11, f32[8,512,128]{2,1,0:T(8,128)} %param.9), kind=kLoop, calls=%fused_computation.7 | loop fusion | flops 2097152 | bytes 6293504 | tf_op jit(solution)/shard_map/convert_element_type | solution.py:39
  5.0 7.3 %all-to-all-start = ((bf16[8,512,256]{2,1,0:T(8,128)(2,1)}), bf16[8,512,256]{2,1,0:T(8,128)(2,1)S(1)}, u32[]{:S(2)}, u32[]{:S(2)}) async-start(bf16[8,512,256]{2,1,0:T(8,128)(2,1)} %pad_maximum_fusion), calls=%async_computation | async-start | bytes 4194304 | tf_op jit(solution)/shard_map/all_to_all | solution.py:41
  12.3 2.8 %convert_element_type.60 = bf16[8,512,128]{2,1,0:T(8,128)(2,1)} convert(f32[8,512,128]{2,1,0:T(8,128)} %param.10) | non-fusion elementwise | flops 524288 | bytes 3145728 | tf_op jit(solution)/shard_map/convert_element_type | solution.py:42
  15.3 6.6 %psum.7 = f32[384]{0:T(512)S(1)} all-reduce(f32[384]{0:T(512)S(1)} %fusion.1), channel_id=1, replica_groups=mesh['fs'=8,'tp'=4] {'tp'}, use_global_device_ids=true, to_apply=%region_4.5 | all-reduce | flops 384 | bytes 3072 | tf_op jit(solution)/shard_map/psum | solution.py:48
  22.0 38.5 %all-to-all-done = bf16[8,512,256]{2,1,0:T(8,128)(2,1)S(1)} async-done(((bf16[8,512,256]{2,1,0:T(8,128)(2,1)}), bf16[8,512,256]{2,1,0:T(8,128)(2,1)S(1)}, u32[]{:S(2)}, u32[]{:S(2)}) %all-to-all-start) | async-done | bytes 2097184 | tf_op jit(solution)/shard_map/all_to_all | solution.py:41
  60.5 3.6 %all-to-all-start.1 = ((bf16[8,512,128]{2,1,0:T(8,128)(2,1)}), bf16[8,512,128]{2,1,0:T(8,128)(2,1)S(1)}, u32[]{:S(2)}, u32[]{:S(2)}) async-start(bf16[8,512,128]{2,1,0:T(8,128)(2,1)} %convert_element_type.60), calls=%async_computation.1 | async-start | bytes 2097152 | tf_op jit(solution)/shard_map/all_to_all | solution.py:43
  71.5 18.9 %collective-permute-done = bf16[2048,256]{1,0:T(8,128)(2,1)} collective-permute-done((bf16[2048,256]{1,0:T(8,128)(2,1)S(1)}, bf16[2048,256]{1,0:T(8,128)(2,1)}, u32[]{:S(2)}, u32[]{:S(2)}) %collective-permute-start) | collective-permute-done | bytes 1048608 | tf_op jit(solution)/shard_map/ppermute | solution.py:75
  90.4 41.6 %all_to_all.44 = bf16[8,96,1024]{2,1,0:T(8,128)(2,1)} all-to-all(bf16[8,96,1024]{2,1,0:T(8,128)(2,1)} %bitcast.66), channel_id=1, replica_groups=mesh['fs'=8,'tp'=4] {'fs'}, dimensions={0} | all-to-all | bytes 3145728 | tf_op jit(solution)/shard_map/all_to_all | solution.py:85
  132.0 4.3 %all-to-all-start.3 = ((bf16[8,96,1024]{2,1,0:T(8,128)(2,1)}), bf16[8,96,1024]{2,1,0:T(8,128)(2,1)}, u32[]{:S(2)}, u32[]{:S(2)}) async-start(bf16[8,96,1024]{2,1,0:T(8,128)(2,1)} %bitcast.65), calls=%async_computation.3 | async-start | bytes 3145728 | tf_op jit(solution)/shard_map/all_to_all | solution.py:85
  144.4 8.0 %collective-permute-done.2 = bf16[768,256]{0,1:T(8,128)(2,1)S(1)} collective-permute-done((bf16[768,256]{0,1:T(8,128)(2,1)S(1)}, bf16[768,256]{0,1:T(8,128)(2,1)S(1)}, u32[]{:S(2)}, u32[]{:S(2)}) %collective-permute-start.2) | collective-permute-done | bytes 393248 | tf_op jit(solution)/shard_map/ppermute | solution.py:117
  156.1 5.0 %collective-permute-done.3 = bf16[768,128]{0,1:T(8,128)(2,1)S(1)} collective-permute-done((bf16[768,128]{0,1:T(8,128)(2,1)S(1)}, bf16[768,128]{0,1:T(8,128)(2,1)S(1)}, u32[]{:S(2)}, u32[]{:S(2)}) %collective-permute-start.3) | collective-permute-done | bytes 196640 | tf_op jit(solution)/shard_map/ppermute | solution.py:120
  163.6 6.2 %collective-permute-done.7 = bf16[1024,128]{1,0:T(8,128)(2,1)S(1)} collective-permute-done((bf16[1024,128]{1,0:T(8,128)(2,1)S(1)}, bf16[1024,128]{1,0:T(8,128)(2,1)S(1)}, u32[]{:S(2)}, u32[]{:S(2)}) %collective-permute-start.7) | collective-permute-done | bytes 262176 | tf_op jit(solution)/shard_map/ppermute | solution.py:103
  169.7 5.9 %collective-permute-done.5 = bf16[1024,128]{1,0:T(8,128)(2,1)S(1)} collective-permute-done((bf16[1024,128]{1,0:T(8,128)(2,1)S(1)}, bf16[1024,128]{1,0:T(8,128)(2,1)S(1)}, u32[]{:S(2)}, u32[]{:S(2)}) %collective-permute-start.5) | collective-permute-done | bytes 262176 | tf_op jit(solution)/shard_map/ppermute | solution.py:103
  178.6 5.3 %all-to-all-start.4 = ((bf16[8,96,1024]{2,1,0:T(8,128)(2,1)}), bf16[8,96,1024]{2,1,0:T(8,128)(2,1)}, u32[]{:S(2)}, u32[]{:S(2)}) async-start(bf16[8,96,1024]{2,1,0:T(8,128)(2,1)} %bitcast.67), calls=%async_computation.4 | async-start | bytes 3145728 | tf_op jit(solution)/shard_map/all_to_all | solution.py:135
  191.9 7.7 %collective-permute-done.9 = bf16[768,256]{0,1:T(8,128)(2,1)S(1)} collective-permute-done((bf16[768,256]{0,1:T(8,128)(2,1)S(1)}, bf16[768,256]{0,1:T(8,128)(2,1)S(1)}, u32[]{:S(2)}, u32[]{:S(2)}) %collective-permute-start.9) | collective-permute-done | bytes 393248 | tf_op jit(solution)/shard_map/ppermute | solution.py:117
  203.4 4.7 %collective-permute-done.10 = bf16[768,128]{0,1:T(8,128)(2,1)S(1)} collective-permute-done((bf16[768,128]{0,1:T(8,128)(2,1)S(1)}, bf16[768,128]{0,1:T(8,128)(2,1)S(1)}, u32[]{:S(2)}, u32[]{:S(2)}) %collective-permute-start.10) | collective-permute-done | bytes 196640 | tf_op jit(solution)/shard_map/ppermute | solution.py:120
  210.0 2.2 convolution_convert_fusion.1
  212.2 9.4 %all-to-all-done.4 = bf16[8,96,1024]{2,1,0:T(8,128)(2,1)} async-done(((bf16[8,96,1024]{2,1,0:T(8,128)(2,1)}), bf16[8,96,1024]{2,1,0:T(8,128)(2,1)}, u32[]{:S(2)}, u32[]{:S(2)}) %all-to-all-start.4) | async-done | bytes 1572896 | tf_op jit(solution)/shard_map/all_to_all | solution.py:135
  221.6 4.4 %all-to-all-start.5 = ((bf16[8,96,1024]{2,1,0:T(8,128)(2,1)}), bf16[8,96,1024]{2,1,0:T(8,128)(2,1)}, u32[]{:S(2)}, u32[]{:S(2)}) async-start(bf16[8,96,1024]{2,1,0:T(8,128)(2,1)} %bitcast.68), calls=%async_computation.5 | async-start | bytes 3145728 | tf_op jit(solution)/shard_map/all_to_all | solution.py:137
  228.6 3.4 %fusion.24 = f32[384,1024]{1,0:T(8,128)} fusion(bf16[768,1024]{1,0:T(8,128)(2,1)} %bitcast.18, bf16[384,1536]{1,0:T(8,128)(2,1)S(1)} %get-tuple-element.23), kind=kOutput, calls=%fused_computation.42 | convolution fusion | flops 603979776 | bytes 3735552 | tf_op jit(solution)/shard_map/dot_general | solution.py:144
  232.0 3.3 %fusion.22 = f32[384,1024]{1,0:T(8,128)} fusion(bf16[768,1024]{1,0:T(8,128)(2,1)} %bitcast.18, bf16[384,1536]{1,0:T(8,128)(2,1)S(1)} %get-tuple-element.22), kind=kOutput, calls=%fused_computation.40 | convolution fusion | flops 603979776 | bytes 3735552 | tf_op jit(solution)/shard_map/dot_general | solution.py:144
  235.3 27.6 %all-to-all-done.5 = bf16[8,96,1024]{2,1,0:T(8,128)(2,1)} async-done(((bf16[8,96,1024]{2,1,0:T(8,128)(2,1)}), bf16[8,96,1024]{2,1,0:T(8,128)(2,1)}, u32[]{:S(2)}, u32[]{:S(2)}) %all-to-all-start.5) | async-done | bytes 1572896 | tf_op jit(solution)/shard_map/all_to_all | solution.py:137
  262.9 2.5 fusion.20
  265.8 3.1 %add_convert_fusion = bf16[384,1024]{1,0:T(8,128)(2,1)} fusion(f32[384,1024]{1,0:T(8,128)S(1)} %fusion.20, f32[384,1024]{1,0:T(8,128)S(1)} %copy-done.4, f32[384,1024]{1,0:T(8,128)S(1)} %copy-done.5, bf16[768,1024]{1,0:T(8,128)(2,1)} %bitcast.21, bf16[384,1536]{1,0:T(8,128)(2,1)S(1)} %copy-done.3), kind=kOutput, calls=%fused_computation.14 | convolution fusion | flops 605552640 | bytes 7667712 | tf_op jit(solution)/shard_map/dot_general | solution.py:144
  (88 shorter events, 43.5 us)
Async XLA Ops:
  5.0 55.5 %all-to-all-start = ((bf16[8,512,256]{2,1,0:T(8,128)(2,1)}), bf16[8,512,256]{2,1,0:T(8,128)(2,1)S(1)}, u32[]{:S(2)}, u32[]{:S(2)}) async-start(bf16[8,512,256]{2,1,0:T(8,128)(2,1)} %pad_maximum_fusion), calls=%async_computation | async-start | bytes 4194304 | tf_op jit(solution)/shard_map/all_to_all | solution.py:41
  12.3 9.7 %copy-start.11 = (s32[384,2]{0,1:T(2,128)S(1)}, s32[384,2]{0,1:T(2,128)}, u32[]{:S(2)}) copy-start(s32[384,2]{0,1:T(2,128)} %param.12) | copy-start | bytes 9220
  60.5 29.9 %all-to-all-start.1 = ((bf16[8,512,128]{2,1,0:T(8,128)(2,1)}), bf16[8,512,128]{2,1,0:T(8,128)(2,1)S(1)}, u32[]{:S(2)}, u32[]{:S(2)}) async-start(bf16[8,512,128]{2,1,0:T(8,128)(2,1)} %convert_element_type.60), calls=%async_computation.1 | async-start | bytes 2097152 | tf_op jit(solution)/shard_map/all_to_all | solution.py:43
  65.5 24.9 %collective-permute-start = (bf16[2048,256]{1,0:T(8,128)(2,1)S(1)}, bf16[2048,256]{1,0:T(8,128)(2,1)}, u32[]{:S(2)}, u32[]{:S(2)}) collective-permute-start(bf16[2048,256]{1,0:T(8,128)(2,1)S(1)} %get-tuple-element.27), channel_id=1, source_target_pairs={{0,2},{1,3},{2,0},{3,1},{4,6},{5,7},{6,4},{7,5},{8,10},{9,11},{10,... | collective-permute-start | bytes 3145736 | tf_op jit(solution)/shard_map/ppermute | solution.py:75
  132.0 6.5 %collective-permute-start.1 = (bf16[768,1024]{1,0:T(8,128)(2,1)}, bf16[768,1024]{1,0:T(8,128)(2,1)}, u32[]{:S(2)}, u32[]{:S(2)}) collective-permute-start(bf16[768,1024]{1,0:T(8,128)(2,1)} %bitcast.5), channel_id=1, source_target_pairs={{0,1},{1,0},{2,3},{3,2},{4,5},{5,4},{6,7},{7,6},{8,9},{9,8},{10,11... | collective-permute-start | bytes 4718600 | tf_op jit(solution)/shard_map/ppermute | solution.py:109
  132.0 46.5 %all-to-all-start.3 = ((bf16[8,96,1024]{2,1,0:T(8,128)(2,1)}), bf16[8,96,1024]{2,1,0:T(8,128)(2,1)}, u32[]{:S(2)}, u32[]{:S(2)}) async-start(bf16[8,96,1024]{2,1,0:T(8,128)(2,1)} %bitcast.65), calls=%async_computation.3 | async-start | bytes 3145728 | tf_op jit(solution)/shard_map/all_to_all | solution.py:85
  140.8 11.6 %collective-permute-start.2 = (bf16[768,256]{0,1:T(8,128)(2,1)S(1)}, bf16[768,256]{0,1:T(8,128)(2,1)S(1)}, u32[]{:S(2)}, u32[]{:S(2)}) collective-permute-start(bf16[768,256]{0,1:T(8,128)(2,1)S(1)} %fusion.5), channel_id=1, source_target_pairs={{0,2},{1,3},{2,0},{3,1},{4,6},{5,7},{6,4},{7,5},{8,10},{9,11},{10,... | collective-permute-start | bytes 1179656 | tf_op jit(solution)/shard_map/ppermute | solution.py:117
  154.5 6.6 %collective-permute-start.3 = (bf16[768,128]{0,1:T(8,128)(2,1)S(1)}, bf16[768,128]{0,1:T(8,128)(2,1)S(1)}, u32[]{:S(2)}, u32[]{:S(2)}) collective-permute-start(bf16[768,128]{0,1:T(8,128)(2,1)S(1)} %fusion.47), channel_id=1, source_target_pairs={{0,2},{1,3},{2,0},{3,1},{4,6},{5,7},{6,4},{7,5},{8,10},{9,11},{10,... | collective-permute-start | bytes 589832 | tf_op jit(solution)/shard_map/ppermute | solution.py:120
  161.2 14.5 %collective-permute-start.4 = (bf16[768,256]{0,1:T(8,128)(2,1)S(1)}, bf16[768,256]{0,1:T(8,128)(2,1)S(1)}, u32[]{:S(2)}, u32[]{:S(2)}) collective-permute-start(bf16[768,256]{0,1:T(8,128)(2,1)S(1)} %pad_maximum_fusion.2), channel_id=1, source_target_pairs={{0,1},{1,0},{2,3},{3,2},{4,5},{5,4},{6,7},{7,6},{8,9},{9,8},{10,11... | collective-permute-start | bytes 1179656 | tf_op jit(solution)/shard_map/ppermute | solution.py:121
  161.3 14.3 %copy-start.9 = (bf16[1024,128]{1,0:T(8,128)(2,1)}, bf16[1024,128]{1,0:T(8,128)(2,1)S(1)}, u32[]{:S(2)}) copy-start(bf16[1024,128]{1,0:T(8,128)(2,1)S(1)} %get-tuple-element.30) | copy-start | bytes 786436
  161.4 8.4 %collective-permute-start.7 = (bf16[1024,128]{1,0:T(8,128)(2,1)S(1)}, bf16[1024,128]{1,0:T(8,128)(2,1)S(1)}, u32[]{:S(2)}, u32[]{:S(2)}) collective-permute-start(bf16[1024,128]{1,0:T(8,128)(2,1)S(1)} %get-tuple-element.31), channel_id=1, source_target_pairs={{0,3},{1,2},{2,1},{3,0},{4,7},{5,6},{6,5},{7,4},{8,11},{9,10},{10,... | collective-permute-start | bytes 786440 | tf_op jit(solution)/shard_map/ppermute | solution.py:103
  163.0 6.7 %collective-permute-start.6 = (bf16[1024,128]{1,0:T(8,128)(2,1)S(1)}, bf16[1024,128]{1,0:T(8,128)(2,1)S(1)}, u32[]{:S(2)}, u32[]{:S(2)}) collective-permute-start(bf16[1024,128]{1,0:T(8,128)(2,1)S(1)} %get-tuple-element.32), channel_id=1, source_target_pairs={{0,1},{1,0},{2,3},{3,2},{4,5},{5,4},{6,7},{7,6},{8,9},{9,8},{10,11... | collective-permute-start | bytes 786440 | tf_op jit(solution)/shard_map/ppermute | solution.py:103
  163.0 12.6 %collective-permute-start.5 = (bf16[1024,128]{1,0:T(8,128)(2,1)S(1)}, bf16[1024,128]{1,0:T(8,128)(2,1)S(1)}, u32[]{:S(2)}, u32[]{:S(2)}) collective-permute-start(bf16[1024,128]{1,0:T(8,128)(2,1)S(1)} %get-tuple-element.33), channel_id=1, source_target_pairs={{0,2},{1,3},{2,0},{3,1},{4,6},{5,7},{6,4},{7,5},{8,10},{9,11},{10,... | collective-permute-start | bytes 786440 | tf_op jit(solution)/shard_map/ppermute | solution.py:103
  169.7 5.9 %copy-start.15 = (bf16[1024,128]{1,0:T(8,128)(2,1)}, bf16[1024,128]{1,0:T(8,128)(2,1)S(1)}, u32[]{:S(2)}) copy-start(bf16[1024,128]{1,0:T(8,128)(2,1)S(1)} %collective-permute-done.6) | copy-start | bytes 786436
  178.6 7.5 %collective-permute-start.8 = (bf16[768,1024]{1,0:T(8,128)(2,1)}, bf16[768,1024]{1,0:T(8,128)(2,1)}, u32[]{:S(2)}, u32[]{:S(2)}) collective-permute-start(bf16[768,1024]{1,0:T(8,128)(2,1)} %bitcast.19), channel_id=1, source_target_pairs={{0,1},{1,0},{2,3},{3,2},{4,5},{5,4},{6,7},{7,6},{8,9},{9,8},{10,11... | collective-permute-start | bytes 4718600 | tf_op jit(solution)/shard_map/ppermute | solution.py:109
  178.6 43.1 %all-to-all-start.4 = ((bf16[8,96,1024]{2,1,0:T(8,128)(2,1)}), bf16[8,96,1024]{2,1,0:T(8,128)(2,1)}, u32[]{:S(2)}, u32[]{:S(2)}) async-start(bf16[8,96,1024]{2,1,0:T(8,128)(2,1)} %bitcast.67), calls=%async_computation.4 | async-start | bytes 3145728 | tf_op jit(solution)/shard_map/all_to_all | solution.py:135
  188.3 11.3 %collective-permute-start.9 = (bf16[768,256]{0,1:T(8,128)(2,1)S(1)}, bf16[768,256]{0,1:T(8,128)(2,1)S(1)}, u32[]{:S(2)}, u32[]{:S(2)}) collective-permute-start(bf16[768,256]{0,1:T(8,128)(2,1)S(1)} %fusion.6), channel_id=1, source_target_pairs={{0,2},{1,3},{2,0},{3,1},{4,6},{5,7},{6,4},{7,5},{8,10},{9,11},{10,... | collective-permute-start | bytes 1179656 | tf_op jit(solution)/shard_map/ppermute | solution.py:117
  201.6 8.3 %copy-start.10 = (bf16[1024,128]{1,0:T(8,128)(2,1)S(1)}, bf16[1024,128]{1,0:T(8,128)(2,1)}, u32[]{:S(2)}) copy-start(bf16[1024,128]{1,0:T(8,128)(2,1)} %copy-done.9) | copy-start | bytes 786436
  201.6 8.3 %copy-start.14 = (bf16[1024,128]{1,0:T(8,128)(2,1)S(1)}, bf16[1024,128]{1,0:T(8,128)(2,1)}, u32[]{:S(2)}) copy-start(bf16[1024,128]{1,0:T(8,128)(2,1)} %copy-done.13) | copy-start | bytes 786436
  201.6 8.3 %copy-start.16 = (bf16[1024,128]{1,0:T(8,128)(2,1)S(1)}, bf16[1024,128]{1,0:T(8,128)(2,1)}, u32[]{:S(2)}) copy-start(bf16[1024,128]{1,0:T(8,128)(2,1)} %copy-done.15) | copy-start | bytes 786436
  201.6 8.3 %copy-start.18 = (bf16[1024,128]{1,0:T(8,128)(2,1)S(1)}, bf16[1024,128]{1,0:T(8,128)(2,1)}, u32[]{:S(2)}) copy-start(bf16[1024,128]{1,0:T(8,128)(2,1)} %copy-done.17) | copy-start | bytes 786436
  201.8 6.3 %collective-permute-start.10 = (bf16[768,128]{0,1:T(8,128)(2,1)S(1)}, bf16[768,128]{0,1:T(8,128)(2,1)S(1)}, u32[]{:S(2)}, u32[]{:S(2)}) collective-permute-start(bf16[768,128]{0,1:T(8,128)(2,1)S(1)} %fusion.46), channel_id=1, source_target_pairs={{0,2},{1,3},{2,0},{3,1},{4,6},{5,7},{6,4},{7,5},{8,10},{9,11},{10,... | collective-permute-start | bytes 589832 | tf_op jit(solution)/shard_map/ppermute | solution.py:120
  208.1 1.8 collective-permute-start.11
  221.6 41.3 %all-to-all-start.5 = ((bf16[8,96,1024]{2,1,0:T(8,128)(2,1)}), bf16[8,96,1024]{2,1,0:T(8,128)(2,1)}, u32[]{:S(2)}, u32[]{:S(2)}) async-start(bf16[8,96,1024]{2,1,0:T(8,128)(2,1)} %bitcast.68), calls=%async_computation.5 | async-start | bytes 3145728 | tf_op jit(solution)/shard_map/all_to_all | solution.py:137
  (12 other events, 39.6 us)

commit v3 on v2

--- a/solution.py
+++ b/solution.py
@@ -35,14 +35,19 @@
     part = capacity // chunks
 
     folded = norm_gain[None, :, None]
-    pair = jnp.concatenate(
-        [(gate_master * folded).astype(jnp.bfloat16), (up_master * folded).astype(jnp.bfloat16)], axis=2
+    trio = jnp.concatenate(
+        [
+            (gate_master * folded).astype(jnp.bfloat16),
+            (up_master * folded).astype(jnp.bfloat16),
+            down_master.astype(jnp.bfloat16),
+        ],
+        axis=2,
     )
-    pair = lax.all_to_all(pair, "fs", split_axis=0, concat_axis=1, tiled=True)
-    down_cast, pair = lax.optimization_barrier((down_master.astype(jnp.bfloat16), pair))
-    down_out = lax.all_to_all(down_cast, "fs", split_axis=0, concat_axis=1, tiled=True)
-    gate_out = pair[:, :, :hidden_cols]
-    up_out = pair[:, :, hidden_cols:]
+    trio = lax.all_to_all(trio, "fs", split_axis=0, concat_axis=1, tiled=True)
+    pair = trio[:, :, : 2 * hidden_cols]
+    gate_out = trio[:, :, :hidden_cols]
+    up_out = trio[:, :, hidden_cols : 2 * hidden_cols]
+    down_out = trio[:, :, 2 * hidden_cols :]
 
     token_float = tokens.astype(jnp.float32)
     sumsquares = lax.psum(jnp.sum(token_float * token_float, axis=1), "tp")
@@ -61,8 +66,7 @@
     where_to = place[:, :, None] == spots
     onehot = jnp.any(where_to, axis=1).astype(jnp.bfloat16)
     mixing = jnp.sum(jnp.where(where_to, mix[:, :, None], 0.0), axis=1)
-    mixing_high = mixing.astype(jnp.bfloat16)
-    mixing_low = (mixing - mixing_high.astype(jnp.float32)).astype(jnp.bfloat16)
+    mixing = mixing.astype(jnp.bfloat16)
     outgoing = lax.dot_general(
         onehot, normed, (((0,), (0,)), ((), ())), preferred_element_type=jnp.float32
     ).astype(jnp.bfloat16)
@@ -79,9 +83,9 @@
     arrived = []
     for c in range(chunks):
         if c == 0:
-            ready, down_out, partner_cols = lax.optimization_barrier((outgoing[c], down_out, partner_cols))
+            ready, trio = lax.optimization_barrier((outgoing[c], trio))
         else:
-            ready, arrived[-1] = lax.optimization_barrier((outgoing[c], last))
+            ready, arrived[-1], partner_cols = lax.optimization_barrier((outgoing[c], last, partner_cols))
         last = lax.all_to_all(ready, "fs", split_axis=0, concat_axis=0, tiled=True)
         arrived.append(last)
 
@@ -139,9 +143,8 @@
     mixed = 0.0
     for c, back in enumerate(returned):
         flat = back.reshape(n_experts * part, width)
-        for weights in (mixing_high, mixing_low):
-            chosen = weights[:, c * n_experts * part : (c + 1) * n_experts * part]
-            mixed = mixed + jnp.dot(chosen, flat, preferred_element_type=jnp.float32)
+        chosen = mixing[:, c * n_experts * part : (c + 1) * n_experts * part]
+        mixed = mixed + jnp.dot(chosen, flat, preferred_element_type=jnp.float32)
     return (gate_out, up_out, down_out, mixed.astype(jnp.bfloat16))
 
 

time: 271 us -> 261 us (0.963)
  blocking collectives: 48.2 us -> 6.62 us
  waiting for transfers between devices: 134 us -> 173 us
  matrix products: 35.6 us -> 29.8 us
    all_to_all x1 -> x0, blocking collectives: 41.6 us -> none  [body(): last = lax.all_to_all(ready, 'fs', split_axis=0, concat_axis=0, tiled=True)]
    all_to_all x2 -> x1, waiting for transfers between devices: 38.6 us -> 56.8 us  [body(): trio = lax.all_to_all(trio, 'fs', split_axis=0, concat_axis=1, tiled=True)]
    all_to_all x1 -> x2, waiting for transfers between devices: 0.01 us -> 11.1 us  [body(): last = lax.all_to_all(ready, 'fs', split_axis=0, concat_axis=0, tiled=True)]
    all_to_all x2, waiting for transfers between devices: 37 us -> 44.6 us  [body(): lax.all_to_all(served, 'fs', split_axis=0, concat_axis=0, tiled=True)]
    dot_general x4 -> x2, matrix products: 12.3 us -> 6.41 us  [body(): mixed = mixed + jnp.dot(chosen, flat, preferred_element_type=jnp.float32)]
    all_to_all x1 -> x2, starting transfers between devices: 4.3 us -> 8.62 us  [body(): last = lax.all_to_all(ready, 'fs', split_axis=0, concat_axis=0, tiled=True)]
    ppermute x1, waiting for transfers between devices: 18.9 us -> 22.7 us  [body(): lax.ppermute(lax.dynamic_slice_in_dim(pair[0], (1 - my_half) * span, span...]
    all_to_all x2 -> x1, starting transfers between devices: 10.9 us -> 7.41 us  [body(): trio = lax.all_to_all(trio, 'fs', split_axis=0, concat_axis=1, tiled=True)]
  transfers between devices with their start and end apart: 17 -> 17, of which waited for: 11 -> 12; matrix products, arithmetic and copies ran while one was open for 15% -> 13% of each run, Pallas kernels for 0% -> 0%
where the time goes in v3:
time: 261 us; the launch traced here: 260 us
  waiting for transfers between devices  173 us (66%)
  starting transfers between devices  35.4 us (14%)
  matrix products  29.8 us (11%)
  other arithmetic  9.17 us (4%)
  blocking collectives  6.62 us (3%)
  local copies, waits for them, and re-layouts  5.51 us (2%)
    all_to_all x1, waiting for transfers between devices, body(): trio = lax.all_to_all(trio, 'fs', split_axis=0, concat_axis=1, tiled=True)  56.8 us
    all_to_all x2, waiting for transfers between devices, body(): lax.all_to_all(served, 'fs', split_axis=0, concat_axis=0, tiled=True)  44.6 us
    ppermute x1, waiting for transfers between devices, body(): lax.ppermute(lax.dynamic_slice_in_dim(pair[0], (1 - my_half) * span, span...  22.7 us
    dot_general x8, matrix products, partial(): total = total + jnp.dot(piece, block, preferred_element_type=jnp.float32)  15.8 us
    ppermute x2, waiting for transfers between devices, serve(): lax.ppermute(partial(partner_blocks).astype(jnp.bfloat16), 'tp', cross_sw...  15.7 us
    ppermute x3, waiting for transfers between devices, body(): piece = lax.ppermute(piece, 'tp', member_shift(j, crossed, n_tp))  12.1 us
    all_to_all x2, waiting for transfers between devices, body(): last = lax.all_to_all(ready, 'fs', split_axis=0, concat_axis=0, tiled=True)  11.1 us
    all_to_all x2, starting transfers between devices, body(): lax.all_to_all(served, 'fs', split_axis=0, concat_axis=0, tiled=True)  9.12 us
  transfers between devices with their start and end apart: 17, of which 12 were waited for; matrix products, arithmetic and copies ran while one was open for 13% of the time, Pallas kernels for 0%

profile of v3, /device:TPU:0, one launch (start us, length us, event | category | flops | bytes accessed | tf_op | source)
XLA Modules:
  0.0 260.0 jit_solution(10696394020961575395)
XLA Ops:
  7.1 7.4 %all-to-all-start = ((bf16[8,512,384]{2,1,0:T(8,128)(2,1)}), bf16[8,512,384]{2,1,0:T(8,128)(2,1)S(1)}, u32[]{:S(2)}, u32[]{:S(2)}) async-start(bf16[8,512,384]{2,1,0:T(8,128)(2,1)} %pad_maximum_fusion), calls=%async_computation | async-start | bytes 6291456 | tf_op jit(solution)/shard_map/all_to_all | solution.py:46
  15.9 6.6 %psum.7 = f32[384]{0:T(512)S(1)} all-reduce(f32[384]{0:T(512)S(1)} %fusion.1), channel_id=1, replica_groups=mesh['fs'=8,'tp'=4] {'tp'}, use_global_device_ids=true, to_apply=%region_6.7 | all-reduce | flops 384 | bytes 3072 | tf_op jit(solution)/shard_map/psum | solution.py:53
  23.4 3.1 %convolution_convert_fusion = bf16[1536,1024]{1,0:T(8,128)(2,1)S(1)} fusion(pred[384,1536]{1,0:T(8,128)(4,1)S(1)} %fusion, bf16[384,1024]{1,0:T(8,128)(2,1)} %param.7, f32[384]{0:T(512)S(1)} %add_rsqrt_fusion), kind=kOutput, calls=%fused_computation.3 | convolution fusion | flops 1210712064 | bytes 4523520 | tf_op jit(solution)/shard_map/dot_general | solution.py:70
  28.4 56.8 %all-to-all-done = bf16[8,512,384]{2,1,0:T(8,128)(2,1)S(1)} async-done(((bf16[8,512,384]{2,1,0:T(8,128)(2,1)}), bf16[8,512,384]{2,1,0:T(8,128)(2,1)S(1)}, u32[]{:S(2)}, u32[]{:S(2)}) %all-to-all-start) | async-done | bytes 3145760 | tf_op jit(solution)/shard_map/all_to_all | solution.py:46
  85.2 4.3 %all-to-all-start.1 = ((bf16[8,96,1024]{2,1,0:T(8,128)(2,1)}), bf16[8,96,1024]{2,1,0:T(8,128)(2,1)}, u32[]{:S(2)}, u32[]{:S(2)}) async-start(bf16[8,96,1024]{2,1,0:T(8,128)(2,1)} %bitcast.62), calls=%async_computation.1 | async-start | bytes 3145728 | tf_op jit(solution)/shard_map/all_to_all | solution.py:89
  92.4 22.7 %collective-permute-done = bf16[2048,256]{1,0:T(8,128)(2,1)} collective-permute-done((bf16[2048,256]{1,0:T(8,128)(2,1)S(1)}, bf16[2048,256]{1,0:T(8,128)(2,1)}, u32[]{:S(2)}, u32[]{:S(2)}) %collective-permute-start) | collective-permute-done | bytes 1048608 | tf_op jit(solution)/shard_map/ppermute | solution.py:79
  115.1 11.1 %all-to-all-done.1 = bf16[8,96,1024]{2,1,0:T(8,128)(2,1)} async-done(((bf16[8,96,1024]{2,1,0:T(8,128)(2,1)}), bf16[8,96,1024]{2,1,0:T(8,128)(2,1)}, u32[]{:S(2)}, u32[]{:S(2)}) %all-to-all-start.1) | async-done | bytes 1572896 | tf_op jit(solution)/shard_map/all_to_all | solution.py:89
  126.2 4.3 %all-to-all-start.2 = ((bf16[8,96,1024]{2,1,0:T(8,128)(2,1)}), bf16[8,96,1024]{2,1,0:T(8,128)(2,1)}, u32[]{:S(2)}, u32[]{:S(2)}) async-start(bf16[8,96,1024]{2,1,0:T(8,128)(2,1)} %bitcast.61), calls=%async_computation.2 | async-start | bytes 3145728 | tf_op jit(solution)/shard_map/all_to_all | solution.py:89
  132.6 2.9 %fusion.5 = bf16[768,256]{0,1:T(8,128)(2,1)} fusion(f32[768,256]{0,1:T(8,128)S(1)} %fusion.23, bf16[768,1024]{1,0:T(8,128)(2,1)} %bitcast.4, bf16[2,1024,256]{2,1,0:T(8,128)(2,1)} %bitcast.8, s32[]{:T(128)S(6)} %select_n.101), kind=kOutput, calls=%fused_computation.20 | convolution fusion | flops 403046400 | bytes 3276804 | tf_op jit(solution)/shard_map/dot_general | solution.py:118
  137.1 2.2 fusion.29
  139.3 8.0 %collective-permute-done.2 = bf16[768,256]{0,1:T(8,128)(2,1)S(1)} collective-permute-done((bf16[768,256]{0,1:T(8,128)(2,1)}, bf16[768,256]{0,1:T(8,128)(2,1)S(1)}, u32[]{:S(2)}, u32[]{:S(2)}) %collective-permute-start.2) | collective-permute-done | bytes 393248 | tf_op jit(solution)/shard_map/ppermute | solution.py:121
  152.9 3.2 %collective-permute-done.3 = bf16[768,128]{0,1:T(8,128)(2,1)S(1)} collective-permute-done((bf16[768,128]{0,1:T(8,128)(2,1)S(1)}, bf16[768,128]{0,1:T(8,128)(2,1)S(1)}, u32[]{:S(2)}, u32[]{:S(2)}) %collective-permute-start.3) | collective-permute-done | bytes 196640 | tf_op jit(solution)/shard_map/ppermute | solution.py:124
  158.5 6.2 %collective-permute-done.7 = bf16[1024,128]{1,0:T(8,128)(2,1)S(1)} collective-permute-done((bf16[1024,128]{1,0:T(8,128)(2,1)S(1)}, bf16[1024,128]{1,0:T(8,128)(2,1)S(1)}, u32[]{:S(2)}, u32[]{:S(2)}) %collective-permute-start.7) | collective-permute-done | bytes 262176 | tf_op jit(solution)/shard_map/ppermute | solution.py:107
  164.7 5.9 %collective-permute-done.5 = bf16[1024,128]{1,0:T(8,128)(2,1)S(1)} collective-permute-done((bf16[1024,128]{1,0:T(8,128)(2,1)S(1)}, bf16[1024,128]{1,0:T(8,128)(2,1)S(1)}, u32[]{:S(2)}, u32[]{:S(2)}) %collective-permute-start.5) | collective-permute-done | bytes 262176 | tf_op jit(solution)/shard_map/ppermute | solution.py:107
  170.6 2.2 convolution_convert_fusion.2
  172.9 5.4 %all-to-all-start.3 = ((bf16[8,96,1024]{2,1,0:T(8,128)(2,1)}), bf16[8,96,1024]{2,1,0:T(8,128)(2,1)}, u32[]{:S(2)}, u32[]{:S(2)}) async-start(bf16[8,96,1024]{2,1,0:T(8,128)(2,1)} %bitcast.64), calls=%async_computation.3 | async-start | bytes 3145728 | tf_op jit(solution)/shard_map/all_to_all | solution.py:139
  185.8 7.7 %collective-permute-done.9 = bf16[768,256]{0,1:T(8,128)(2,1)S(1)} collective-permute-done((bf16[768,256]{0,1:T(8,128)(2,1)S(1)}, bf16[768,256]{0,1:T(8,128)(2,1)S(1)}, u32[]{:S(2)}, u32[]{:S(2)}) %collective-permute-start.9) | collective-permute-done | bytes 393248 | tf_op jit(solution)/shard_map/ppermute | solution.py:121
  195.8 4.7 %collective-permute-done.10 = bf16[768,128]{0,1:T(8,128)(2,1)S(1)} collective-permute-done((bf16[768,128]{0,1:T(8,128)(2,1)S(1)}, bf16[768,128]{0,1:T(8,128)(2,1)S(1)}, u32[]{:S(2)}, u32[]{:S(2)}) %collective-permute-start.10) | collective-permute-done | bytes 196640 | tf_op jit(solution)/shard_map/ppermute | solution.py:124
  202.4 2.2 convolution_convert_fusion.1
  204.6 11.4 %all-to-all-done.3 = bf16[8,96,1024]{2,1,0:T(8,128)(2,1)} async-done(((bf16[8,96,1024]{2,1,0:T(8,128)(2,1)}), bf16[8,96,1024]{2,1,0:T(8,128)(2,1)}, u32[]{:S(2)}, u32[]{:S(2)}) %all-to-all-start.3) | async-done | bytes 1572896 | tf_op jit(solution)/shard_map/all_to_all | solution.py:139
  216.0 3.8 %all-to-all-start.4 = ((bf16[8,96,1024]{2,1,0:T(8,128)(2,1)}), bf16[8,96,1024]{2,1,0:T(8,128)(2,1)S(1)}, u32[]{:S(2)}, u32[]{:S(2)}) async-start(bf16[8,96,1024]{2,1,0:T(8,128)(2,1)} %bitcast.19), calls=%async_computation.4 | async-start | bytes 3145728 | tf_op jit(solution)/shard_map/all_to_all | solution.py:141
  220.4 3.3 %fusion.20 = f32[384,1024]{1,0:T(8,128)} fusion(bf16[768,1024]{1,0:T(8,128)(2,1)} %bitcast.17, bf16[384,1536]{1,0:T(8,128)(2,1)S(1)} %select_reduce_fusion), kind=kOutput, calls=%fused_computation.37 | convolution fusion | flops 603979776 | bytes 3735552 | tf_op jit(solution)/shard_map/dot_general | solution.py:147
  223.8 33.2 %all-to-all-done.4 = bf16[8,96,1024]{2,1,0:T(8,128)(2,1)S(1)} async-done(((bf16[8,96,1024]{2,1,0:T(8,128)(2,1)}), bf16[8,96,1024]{2,1,0:T(8,128)(2,1)S(1)}, u32[]{:S(2)}, u32[]{:S(2)}) %all-to-all-start.4) | async-done | bytes 1572896 | tf_op jit(solution)/shard_map/all_to_all | solution.py:141
  257.0 3.1 %add_convert_fusion = bf16[384,1024]{1,0:T(8,128)(2,1)} fusion(f32[384,1024]{1,0:T(8,128)} %fusion.20, bf16[768,1024]{1,0:T(8,128)(2,1)S(1)} %bitcast.60, bf16[384,1536]{1,0:T(8,128)(2,1)S(1)} %select_reduce_fusion), kind=kOutput, calls=%fused_computation.13 | convolution fusion | flops 604766208 | bytes 4521984 | tf_op jit(solution)/shard_map/dot_general | solution.py:147
  (72 shorter events, 37.5 us)
Async XLA Ops:
  7.1 15.4 %copy-start.4 = (s32[384,2]{0,1:T(2,128)S(1)}, s32[384,2]{0,1:T(2,128)}, u32[]{:S(2)}) copy-start(s32[384,2]{0,1:T(2,128)} %param.12) | copy-start | bytes 9220
  7.1 78.1 %all-to-all-start = ((bf16[8,512,384]{2,1,0:T(8,128)(2,1)}), bf16[8,512,384]{2,1,0:T(8,128)(2,1)S(1)}, u32[]{:S(2)}, u32[]{:S(2)}) async-start(bf16[8,512,384]{2,1,0:T(8,128)(2,1)} %pad_maximum_fusion), calls=%async_computation | async-start | bytes 6291456 | tf_op jit(solution)/shard_map/all_to_all | solution.py:46
  85.2 40.9 %all-to-all-start.1 = ((bf16[8,96,1024]{2,1,0:T(8,128)(2,1)}), bf16[8,96,1024]{2,1,0:T(8,128)(2,1)}, u32[]{:S(2)}, u32[]{:S(2)}) async-start(bf16[8,96,1024]{2,1,0:T(8,128)(2,1)} %bitcast.62), calls=%async_computation.1 | async-start | bytes 3145728 | tf_op jit(solution)/shard_map/all_to_all | solution.py:89
  90.9 24.2 %collective-permute-start = (bf16[2048,256]{1,0:T(8,128)(2,1)S(1)}, bf16[2048,256]{1,0:T(8,128)(2,1)}, u32[]{:S(2)}, u32[]{:S(2)}) collective-permute-start(bf16[2048,256]{1,0:T(8,128)(2,1)S(1)} %get-tuple-element.22), channel_id=1, source_target_pairs={{0,2},{1,3},{2,0},{3,1},{4,6},{5,7},{6,4},{7,5},{8,10},{9,11},{10,... | collective-permute-start | bytes 3145736 | tf_op jit(solution)/shard_map/ppermute | solution.py:79
  126.2 4.3 %collective-permute-start.1 = (bf16[768,1024]{1,0:T(8,128)(2,1)}, bf16[768,1024]{1,0:T(8,128)(2,1)}, u32[]{:S(2)}, u32[]{:S(2)}) collective-permute-start(bf16[768,1024]{1,0:T(8,128)(2,1)} %bitcast.4), channel_id=1, source_target_pairs={{0,1},{1,0},{2,3},{3,2},{4,5},{5,4},{6,7},{7,6},{8,9},{9,8},{10,11... | collective-permute-start | bytes 4718600 | tf_op jit(solution)/shard_map/ppermute | solution.py:113
  126.2 46.6 %all-to-all-start.2 = ((bf16[8,96,1024]{2,1,0:T(8,128)(2,1)}), bf16[8,96,1024]{2,1,0:T(8,128)(2,1)}, u32[]{:S(2)}, u32[]{:S(2)}) async-start(bf16[8,96,1024]{2,1,0:T(8,128)(2,1)} %bitcast.61), calls=%async_computation.2 | async-start | bytes 3145728 | tf_op jit(solution)/shard_map/all_to_all | solution.py:89
  135.5 11.7 %collective-permute-start.2 = (bf16[768,256]{0,1:T(8,128)(2,1)}, bf16[768,256]{0,1:T(8,128)(2,1)S(1)}, u32[]{:S(2)}, u32[]{:S(2)}) collective-permute-start(bf16[768,256]{0,1:T(8,128)(2,1)} %fusion.5), channel_id=1, source_target_pairs={{0,2},{1,3},{2,0},{3,1},{4,6},{5,7},{6,4},{7,5},{8,10},{9,11},{10,... | collective-permute-start | bytes 1179656 | tf_op jit(solution)/shard_map/ppermute | solution.py:121
  137.1 10.2 %copy-start = (bf16[1,2048,256]{2,1,0:T(8,128)(2,1)S(1)}, bf16[1,2048,256]{2,1,0:T(8,128)(2,1)}, u32[]{:S(2)}) copy-start(bf16[1,2048,256]{2,1,0:T(8,128)(2,1)} %get-tuple-element.21) | copy-start | bytes 3145732
  149.5 6.6 %collective-permute-start.3 = (bf16[768,128]{0,1:T(8,128)(2,1)S(1)}, bf16[768,128]{0,1:T(8,128)(2,1)S(1)}, u32[]{:S(2)}, u32[]{:S(2)}) collective-permute-start(bf16[768,128]{0,1:T(8,128)(2,1)S(1)} %fusion.43), channel_id=1, source_target_pairs={{0,2},{1,3},{2,0},{3,1},{4,6},{5,7},{6,4},{7,5},{8,10},{9,11},{10,... | collective-permute-start | bytes 589832 | tf_op jit(solution)/shard_map/ppermute | solution.py:124
  156.1 14.5 %collective-permute-start.4 = (bf16[768,256]{0,1:T(8,128)(2,1)S(1)}, bf16[768,256]{0,1:T(8,128)(2,1)S(1)}, u32[]{:S(2)}, u32[]{:S(2)}) collective-permute-start(bf16[768,256]{0,1:T(8,128)(2,1)S(1)} %pad_maximum_fusion.2), channel_id=1, source_target_pairs={{0,1},{1,0},{2,3},{3,2},{4,5},{5,4},{6,7},{7,6},{8,9},{9,8},{10,11... | collective-permute-start | bytes 1179656 | tf_op jit(solution)/shard_map/ppermute | solution.py:125
  156.3 8.4 %collective-permute-start.7 = (bf16[1024,128]{1,0:T(8,128)(2,1)S(1)}, bf16[1024,128]{1,0:T(8,128)(2,1)S(1)}, u32[]{:S(2)}, u32[]{:S(2)}) collective-permute-start(bf16[1024,128]{1,0:T(8,128)(2,1)S(1)} %get-tuple-element.24), channel_id=1, source_target_pairs={{0,3},{1,2},{2,1},{3,0},{4,7},{5,6},{6,5},{7,4},{8,11},{9,10},{10,... | collective-permute-start | bytes 786440 | tf_op jit(solution)/shard_map/ppermute | solution.py:107
  158.0 6.7 %collective-permute-start.6 = (bf16[1024,128]{1,0:T(8,128)(2,1)S(1)}, bf16[1024,128]{1,0:T(8,128)(2,1)S(1)}, u32[]{:S(2)}, u32[]{:S(2)}) collective-permute-start(bf16[1024,128]{1,0:T(8,128)(2,1)S(1)} %get-tuple-element.25), channel_id=1, source_target_pairs={{0,1},{1,0},{2,3},{3,2},{4,5},{5,4},{6,7},{7,6},{8,9},{9,8},{10,11... | collective-permute-start | bytes 786440 | tf_op jit(solution)/shard_map/ppermute | solution.py:107
  158.0 12.6 %collective-permute-start.5 = (bf16[1024,128]{1,0:T(8,128)(2,1)S(1)}, bf16[1024,128]{1,0:T(8,128)(2,1)S(1)}, u32[]{:S(2)}, u32[]{:S(2)}) collective-permute-start(bf16[1024,128]{1,0:T(8,128)(2,1)S(1)} %get-tuple-element.26), channel_id=1, source_target_pairs={{0,2},{1,3},{2,0},{3,1},{4,6},{5,7},{6,4},{7,5},{8,10},{9,11},{10,... | collective-permute-start | bytes 786440 | tf_op jit(solution)/shard_map/ppermute | solution.py:107
  164.7 8.1 %copy-start.7 = (bf16[1024,128]{1,0:T(8,128)(2,1)}, bf16[1024,128]{1,0:T(8,128)(2,1)S(1)}, u32[]{:S(2)}) copy-start(bf16[1024,128]{1,0:T(8,128)(2,1)S(1)} %collective-permute-done.7) | copy-start | bytes 786436
  164.7 8.1 %copy-start.9 = (bf16[1024,128]{1,0:T(8,128)(2,1)}, bf16[1024,128]{1,0:T(8,128)(2,1)S(1)}, u32[]{:S(2)}) copy-start(bf16[1024,128]{1,0:T(8,128)(2,1)S(1)} %collective-permute-done.6) | copy-start | bytes 786436
  172.8 7.6 %collective-permute-start.8 = (bf16[768,1024]{1,0:T(8,128)(2,1)}, bf16[768,1024]{1,0:T(8,128)(2,1)S(1)}, u32[]{:S(2)}, u32[]{:S(2)}) collective-permute-start(bf16[768,1024]{1,0:T(8,128)(2,1)} %bitcast.18), channel_id=1, source_target_pairs={{0,1},{1,0},{2,3},{3,2},{4,5},{5,4},{6,7},{7,6},{8,9},{9,8},{10,11... | collective-permute-start | bytes 4718600 | tf_op jit(solution)/shard_map/ppermute | solution.py:113
  172.9 43.1 %all-to-all-start.3 = ((bf16[8,96,1024]{2,1,0:T(8,128)(2,1)}), bf16[8,96,1024]{2,1,0:T(8,128)(2,1)}, u32[]{:S(2)}, u32[]{:S(2)}) async-start(bf16[8,96,1024]{2,1,0:T(8,128)(2,1)} %bitcast.64), calls=%async_computation.3 | async-start | bytes 3145728 | tf_op jit(solution)/shard_map/all_to_all | solution.py:139
  182.1 11.3 %collective-permute-start.9 = (bf16[768,256]{0,1:T(8,128)(2,1)S(1)}, bf16[768,256]{0,1:T(8,128)(2,1)S(1)}, u32[]{:S(2)}, u32[]{:S(2)}) collective-permute-start(bf16[768,256]{0,1:T(8,128)(2,1)S(1)} %fusion.6), channel_id=1, source_target_pairs={{0,2},{1,3},{2,0},{3,1},{4,6},{5,7},{6,4},{7,5},{8,10},{9,11},{10,... | collective-permute-start | bytes 1179656 | tf_op jit(solution)/shard_map/ppermute | solution.py:121
  194.1 8.3 %copy-start.8 = (bf16[1024,128]{1,0:T(8,128)(2,1)S(1)}, bf16[1024,128]{1,0:T(8,128)(2,1)}, u32[]{:S(2)}) copy-start(bf16[1024,128]{1,0:T(8,128)(2,1)} %copy-done.7) | copy-start | bytes 786436
  194.1 8.3 %copy-start.10 = (bf16[1024,128]{1,0:T(8,128)(2,1)S(1)}, bf16[1024,128]{1,0:T(8,128)(2,1)}, u32[]{:S(2)}) copy-start(bf16[1024,128]{1,0:T(8,128)(2,1)} %copy-done.9) | copy-start | bytes 786436
  194.1 8.3 %copy-start.12 = (bf16[1024,128]{1,0:T(8,128)(2,1)S(1)}, bf16[1024,128]{1,0:T(8,128)(2,1)}, u32[]{:S(2)}) copy-start(bf16[1024,128]{1,0:T(8,128)(2,1)} %copy-done.11) | copy-start | bytes 786436
  194.2 6.3 %collective-permute-start.10 = (bf16[768,128]{0,1:T(8,128)(2,1)S(1)}, bf16[768,128]{0,1:T(8,128)(2,1)S(1)}, u32[]{:S(2)}, u32[]{:S(2)}) collective-permute-start(bf16[768,128]{0,1:T(8,128)(2,1)S(1)} %fusion.42), channel_id=1, source_target_pairs={{0,2},{1,3},{2,0},{3,1},{4,6},{5,7},{6,4},{7,5},{8,10},{9,11},{10,... | collective-permute-start | bytes 589832 | tf_op jit(solution)/shard_map/ppermute | solution.py:124
  200.6 1.8 collective-permute-start.11
  216.0 41.0 %all-to-all-start.4 = ((bf16[8,96,1024]{2,1,0:T(8,128)(2,1)}), bf16[8,96,1024]{2,1,0:T(8,128)(2,1)S(1)}, u32[]{:S(2)}, u32[]{:S(2)}) async-start(bf16[8,96,1024]{2,1,0:T(8,128)(2,1)} %bitcast.19), calls=%async_computation.4 | async-start | bytes 3145728 | tf_op jit(solution)/shard_map/all_to_all | solution.py:141
  (6 other events, 17.1 us)
